TPU v7x, 32 devices: a whole 2x2x4 slice. The times are simulated.
32 devices in a mesh: grp: 2 (over y), ep: 4 (over z), tp: 4 (over x, core).
Axes of the slice: x: 2, y: 2, z: 4, core: 2. Of those that a mesh axis runs over, the one named last changes fastest.
Arguments:
- tokens: bfloat16 [2048, 2048], P(('grp', 'ep')), parts along dimension 0, may hold values from -6 to 6
- norm_gain: float32 [2048], replicated, may hold values from 0.1 to 1.9
- routing: int32 [2048, 2], P(('grp', 'ep')), parts along dimension 0, may hold values from 0 to 3, all different within a row; in each aligned block of 256 rows (0 to 255, 256 to 511, ...) at most 192 rows name the same one
- gate_weights: float32 [2048, 2], P(('grp', 'ep')), parts along dimension 0, may hold values from 0.2 to 2
- expert_gate: bfloat16 [4, 2048, 1024], P('ep', None, 'tp'), may hold values from -0.125 to 0.125
- expert_up: bfloat16 [4, 2048, 1024], P('ep', None, 'tp'), may hold values from -0.125 to 0.125
- expert_down: bfloat16 [4, 1024, 2048], P('ep', 'tp'), may hold values from -0.1875 to 0.1875
- shared_gate: bfloat16 [2048, 512], P(None, 'tp'), may hold values from -0.125 to 0.125
- shared_up: bfloat16 [2048, 512], P(None, 'tp'), may hold values from -0.125 to 0.125
- shared_down: bfloat16 [512, 2048], P('tp'), may hold values from -0.25 to 0.25
Outputs:
- mixed: bfloat16 [2048, 2048], P(('grp', 'ep'), 'tp'), parts along dimension 0
There are 2 independent parts, one for each index of `grp`. A program takes and returns all parts, laid end to end along the dimension named above; an argument that names none is the same for every part. Nothing has to cross between parts.
Inputs may be any that keep to these rules, and one draw needn't show every extreme that they name: `routing`: each row names 2 different experts. Within each aligned block of 256 rows no expert is named by more than 192 rows, and in every draw some block has an expert named by exactly 192 rows.
All inputs are finite; a program needn't handle non-finite values.
Results may differ from a plain program's by a relative error of at most 0.012.
Values may be sent and summed in bfloat16 or wider, within the bound.
No kernel may reach another device: no remote copies, remote signals or barrier semaphores. Data moves between devices by JAX's collectives and lax.ppermute only.
A program may use at most 64 MiB of HBM per device.

v0:
```python
import jax
import jax.numpy as jnp
from jax import lax
from jax.sharding import PartitionSpec as P


def norm_rows(tokens, norm_gain):
    values = tokens.astype(jnp.float32)
    scale = lax.rsqrt(jnp.mean(values * values, axis=-1, keepdims=True) + 1e-06)
    return (values * scale * norm_gain).astype(jnp.bfloat16)


def body(
    tokens,
    norm_gain,
    routing,
    gate_weights,
    expert_gate,
    expert_up,
    expert_down,
    shared_gate,
    shared_up,
    shared_down,
):
    ep_count = lax.axis_size("ep")
    tp_count = lax.axis_size("tp")
    tok_rows, width = tokens.shape
    top = routing.shape[1]
    local_experts = expert_gate.shape[0]
    experts = ep_count * local_experts
    capacity = max(2, 3 * tok_rows * top // (2 * experts))
    quarter = width // tp_count
    arrived_rows = ep_count * capacity
    normed = norm_rows(tokens, norm_gain)
    flat_experts = routing.reshape(-1)
    assign = flat_experts.shape[0]
    onehot = (flat_experts[:, None] == jnp.arange(experts, dtype=jnp.int32)[None, :]).astype(
        jnp.float32
    )
    lower = (jnp.arange(assign)[:, None] >= jnp.arange(assign)[None, :]).astype(jnp.float32)
    running = jnp.dot(lower, onehot, precision=lax.Precision.HIGHEST)
    slot = (jnp.sum(running * onehot, axis=1) - 1.0).astype(jnp.int32)
    dest = flat_experts * capacity + slot
    owner = jnp.arange(assign, dtype=jnp.int32) // top
    slot_token = jnp.full((experts * capacity,), tok_rows, jnp.int32).at[dest].set(owner)
    padded = jnp.concatenate([normed, jnp.zeros((1, width), jnp.bfloat16)], axis=0)
    outgoing = padded[slot_token].reshape(experts, capacity, width)
    position = lax.axis_index("tp")
    own_columns = lax.dynamic_slice_in_dim(outgoing, position * quarter, quarter, 2)
    arrived = lax.all_to_all(own_columns, "ep", split_axis=0, concat_axis=0, tiled=True)
    piece = lax.all_gather(arrived, "tp", axis=2, tiled=True)
    count = piece.shape[2]
    piece = piece.reshape(ep_count, local_experts, capacity, count)
    local = 0
    rows = piece[:, local].reshape(arrived_rows, count)
    gate_rows = expert_gate[local]
    up_rows = expert_up[local]
    gate_list = [jnp.dot(rows, gate_rows, preferred_element_type=jnp.float32)]
    up_list = [jnp.dot(rows, up_rows, preferred_element_type=jnp.float32)]
    gate_all = jnp.stack(gate_list)
    up_all = jnp.stack(up_list)
    local = 0
    hidden = (jax.nn.silu(gate_all[local]) * up_all[local]).astype(jnp.bfloat16)
    term = jnp.dot(hidden, expert_down[local], preferred_element_type=jnp.float32)
    routed_list = [term.reshape(ep_count, capacity, width)]
    routed_terms = jnp.stack(routed_list, axis=1).reshape(experts * capacity, width)
    shared_gate_rows = jnp.dot(normed, shared_gate, preferred_element_type=jnp.float32)
    shared_up_rows = jnp.dot(normed, shared_up, preferred_element_type=jnp.float32)
    shared_hidden = (jax.nn.silu(shared_gate_rows) * shared_up_rows).astype(jnp.bfloat16)
    shared_term = jnp.dot(shared_hidden, shared_down, preferred_element_type=jnp.float32)
    routed_sum, shared_sum = (
        lax.psum_scatter(
            routed_terms.astype(jnp.bfloat16), "tp", scatter_dimension=1, tiled=True
        ).astype(jnp.float32),
        lax.psum_scatter(
            shared_term.astype(jnp.bfloat16), "tp", scatter_dimension=1, tiled=True
        ).astype(jnp.float32),
    )
    expert_out = routed_sum.astype(jnp.bfloat16).reshape(experts, capacity, quarter)
    returned = lax.all_to_all(expert_out, "ep", split_axis=0, concat_axis=0, tiled=True)
    picked = returned.reshape(experts * capacity, quarter)[dest]
    picked = picked.astype(jnp.float32).reshape(tok_rows, top, quarter)
    routed = jnp.sum(picked * gate_weights[:, :, None], axis=1)
    return (routed + shared_sum).astype(jnp.bfloat16)


def solution(mesh):
    in_specs = (
        P(("grp", "ep"), None),
        P(),
        P(("grp", "ep"), None),
        P(("grp", "ep"), None),
        P("ep", None, "tp"),
        P("ep", None, "tp"),
        P("ep", "tp", None),
        P(None, "tp"),
        P(None, "tp"),
        P("tp", None),
    )
    out_specs = P(("grp", "ep"), "tp")
    return jax.shard_map(body, mesh=mesh, in_specs=in_specs, out_specs=out_specs, check_vma=False)
```

profile of v0, /device:TPU:0, one launch (start us, length us, event | category | flops | bytes accessed | tf_op | source)
XLA Modules:
  0.0 160.1 jit_solution(5352269247419318608)
XLA Ops:
  6.5 0.0 copy-start
  6.5 0.0 all-gather.2.cloned.1.call-start
  6.5 0.8 broadcast_multiply_fusion
  7.3 0.8 copy.13
  8.1 1.5 fusion
  9.7 0.1 copy.12
  9.8 0.1 mul.70
  9.9 0.1 eq.15
  10.1 0.3 fusion.5
  10.4 2.4 %scatter_custom_fusion = s32[768]{0:T(1024)S(1)} fusion(s32[512]{0:T(512)S(1)} %bitcast.27, s32[512]{0:T(512)S(1)} %add_select_fusion, s32[]{:T(128)} %constant.23.clone.1), kind=kCustom, calls=%fused_computation.48 | custom fusion | bytes 3076 | tf_op jit(solution)/shard_map/scatter | solution.py:45
  12.9 1.5 fusion.2
  14.4 0.1 concatenate.3
  14.5 4.3 %gather_fusion = bf16[768,2048]{1,0:T(8,128)(2,1)} fusion(bf16[257,2048]{1,0:T(8,128)(2,1)S(1)} %concatenate.3, s32[1024]{0:T(1024)S(1)} %pad_clamp_fusion.1), kind=kCustom, calls=%fused_computation | custom fusion | bytes 6294528 | tf_op jit(solution)/shard_map/gather | solution.py:47
  18.8 0.0 copy-start.4
  18.8 1.3 constant_dynamic-slice_fusion
  20.1 26.4 %all_to_all.10 = bf16[4,192,512]{2,1,0:T(8,128)(2,1)} all-to-all(bf16[4,192,512]{2,1,0:T(8,128)(2,1)S(1)} %constant_dynamic-slice_fusion), channel_id=1, replica_groups=mesh['grp'=2,'ep'=4,'tp'=4] {'ep'}, dimensions={0} | all-to-all | bytes 1572864 | tf_op jit(solution)/shard_map/all_to_all | solution.py:50
  46.4 0.0 all-gather.2.cloned.1.call-update
  46.5 0.0 reduce-scatter.3.cloned.1.call-start
  46.5 27.7 %all-gather.2.cloned.1.call-done = bf16[4,192,2048]{2,1,0:T(8,128)(2,1)} async-done(((bf16[4,192,512]{2,1,0:T(8,128)(2,1)}), bf16[4,192,2048]{2,1,0:T(8,128)(2,1)}) %all-gather.2.cloned.1.call-update) | async-done | bytes 3145744 | tf_op jit(solution)/shard_map/all_gather | solution.py:51
  74.2 0.0 copy-done.4
  74.2 3.8 %fusion.9 = f32[768,256]{1,0:T(8,128)} fusion(bf16[768,2048]{1,0:T(8,128)(2,1)} %bitcast.30, bf16[1,2048,256]{2,1,0:T(8,128)(2,1)S(1)} %copy-done.4), kind=kOutput, calls=%fused_computation.18 | convolution fusion | flops 805306368 | bytes 4980736 | tf_op jit(solution)/shard_map/dot_general | solution.py:58
  78.0 0.0 copy-done
  78.0 7.4 %convolution_convert_fusion = bf16[768,2048]{1,0:T(8,128)(2,1)} fusion(bf16[768,2048]{1,0:T(8,128)(2,1)} %bitcast.31, bf16[1,256,2048]{2,1,0:T(8,128)(2,1)S(1)} %copy-done, bf16[1,2048,256]{2,1,0:T(8,128)(2,1)} %param.15, f32[768,256]{1,0:T(8,128)} %fusion.9), kind=kOutput, calls=%fused_computation.3 | convolution fusion | flops 1613365248 | bytes 9175040 | tf_op jit(solution)/shard_map/dot_general | solution.py:64
  85.4 0.0 copy-start.1
  85.4 0.0 copy-start.2
  85.4 0.0 reduce-scatter.3.cloned.1.call-update
  85.4 0.0 reduce-scatter.5.cloned.1.call-start
  85.5 1.5 fusion.31
  87.0 0.0 copy-done.1
  87.0 0.0 copy-done.2
  87.0 0.0 copy-start.3
  87.0 1.8 %convolution_convert_fusion.1 = bf16[256,2048]{1,0:T(8,128)(2,1)} fusion(bf16[128,2048]{1,0:T(8,128)(2,1)S(1)} %copy-done.1, bf16[256,2048]{1,0:T(8,128)(2,1)S(1)} %fusion.2, bf16[2048,128]{1,0:T(8,128)(2,1)S(1)} %copy-done.2, f32[256,128]{1,0:T(8,128)S(1)} %fusion.31), kind=kOutput, calls=%fused_computation.6 | convolution fusion | flops 269156352 | bytes 3276800 | tf_op jit(solution)/shard_map/dot_general | solution.py:70
  88.8 0.0 reduce-scatter.5.cloned.1.call-update
  88.8 34.5 %reduce-scatter.3.cloned.1.call-done = bf16[768,512]{1,0:T(8,128)(2,1)} async-done(((bf16[768,2048]{1,0:T(8,128)(2,1)}), bf16[768,512]{1,0:T(8,128)(2,1)}) %reduce-scatter.3.cloned.1.call-update) | async-done | bytes 786448 | tf_op jit(solution)/shard_map/reduce_scatter | solution.py:72
  123.3 4.6 %all-to-all-start.1 = ((bf16[4,192,512]{2,1,0:T(8,128)(2,1)}), bf16[4,192,512]{2,1,0:T(8,128)(2,1)S(1)}, u32[]{:S(2)}, u32[]{:S(2)}) async-start(bf16[4,192,512]{2,1,0:T(8,128)(2,1)} %bitcast.26), calls=%async_computation.2 | async-start | bytes 1572864 | tf_op jit(solution)/shard_map/all_to_all | solution.py:80
  127.9 0.0 copy-done.3
  127.9 0.1 copy.14
  128.0 19.8 %all-to-all-done.1 = bf16[4,192,512]{2,1,0:T(8,128)(2,1)S(1)} async-done(((bf16[4,192,512]{2,1,0:T(8,128)(2,1)}), bf16[4,192,512]{2,1,0:T(8,128)(2,1)S(1)}, u32[]{:S(2)}, u32[]{:S(2)}) %all-to-all-start.1) | async-done | bytes 786464 | tf_op jit(solution)/shard_map/all_to_all | solution.py:80
  147.8 2.0 %gather_fusion.1 = bf16[512,512]{1,0:T(8,128)(2,1)S(1)} fusion(bf16[768,512]{1,0:T(8,128)(2,1)S(1)} %bitcast.24, s32[1024]{0:T(1024)S(1)} %pad_clamp_fusion), kind=kCustom, calls=%fused_computation.1 | custom fusion | bytes 1050624 | tf_op jit(solution)/shard_map/gather | solution.py:81
  149.8 0.7 reshape.65
  150.5 1.3 multiply_reduce_fusion
  151.8 0.0 reduce-scatter.5.cloned.1.call-done
  151.8 1.7 %add_convert_fusion = bf16[256,512]{1,0:T(8,128)(2,1)} fusion(f32[256,512]{1,0:T(8,128)S(1)} %multiply_reduce_fusion, bf16[256,512]{1,0:T(8,128)(2,1)} %reduce-scatter.5.cloned.1.call-done), kind=kLoop, calls=%fused_computation.27 | loop fusion | flops 393216 | bytes 1048576 | tf_op jit(solution)/shard_map/convert_element_type | solution.py:84
  (7 shorter events, 0.0 us)
Async XLA Ops:
  6.5 71.5 %copy-start = (bf16[1,256,2048]{2,1,0:T(8,128)(2,1)S(1)}, bf16[1,256,2048]{2,1,0:T(8,128)(2,1)}, u32[]{:S(2)}) copy-start(bf16[1,256,2048]{2,1,0:T(8,128)(2,1)} %param.16) | copy-start | bytes 3145732
  6.5 67.7 %all-gather.2.cloned.1.call-start = ((), (), s32[]{:S(2)}) async-start(), calls=%async_computation.4 | async-start | bytes 3932160 | tf_op jit(solution)/shard_map/all_gather | solution.py:51
  18.8 55.4 %copy-start.4 = (bf16[1,2048,256]{2,1,0:T(8,128)(2,1)S(1)}, bf16[1,2048,256]{2,1,0:T(8,128)(2,1)}, u32[]{:S(2)}) copy-start(bf16[1,2048,256]{2,1,0:T(8,128)(2,1)} %param.14) | copy-start | bytes 3145732
  46.5 76.8 %reduce-scatter.3.cloned.1.call-start = ((), (), s32[]{:S(2)}) async-start(), calls=%async_computation.5 | async-start | bytes 3932160 | tf_op jit(solution)/shard_map/reduce_scatter | solution.py:72
  85.4 1.6 %copy-start.1 = (bf16[128,2048]{1,0:T(8,128)(2,1)S(1)}, bf16[128,2048]{1,0:T(8,128)(2,1)}, u32[]{:S(2)}) copy-start(bf16[128,2048]{1,0:T(8,128)(2,1)} %param.19) | copy-start | bytes 1572868
  85.4 1.6 %copy-start.2 = (bf16[2048,128]{1,0:T(8,128)(2,1)S(1)}, bf16[2048,128]{1,0:T(8,128)(2,1)}, u32[]{:S(2)}) copy-start(bf16[2048,128]{1,0:T(8,128)(2,1)} %param.18) | copy-start | bytes 1572868
  85.4 66.4 %reduce-scatter.5.cloned.1.call-start = ((), (), s32[]{:S(2)}) async-start(), calls=%async_computation.6 | async-start | bytes 1310720 | tf_op jit(solution)/shard_map/reduce_scatter | solution.py:75
  87.0 40.9 %copy-start.3 = (f32[256,2]{0,1:T(2,128)S(1)}, f32[256,2]{0,1:T(2,128)}, u32[]{:S(2)}) copy-start(f32[256,2]{0,1:T(2,128)} %param.13) | copy-start | bytes 6148
  123.3 24.5 %all-to-all-start.1 = ((bf16[4,192,512]{2,1,0:T(8,128)(2,1)}), bf16[4,192,512]{2,1,0:T(8,128)(2,1)S(1)}, u32[]{:S(2)}, u32[]{:S(2)}) async-start(bf16[4,192,512]{2,1,0:T(8,128)(2,1)} %bitcast.26), calls=%async_computation.2 | async-start | bytes 1572864 | tf_op jit(solution)/shard_map/all_to_all | solution.py:80
Sparse Core Ops, SparseCore 0:
  46.6 27.6 all-gather.1
  85.5 37.7 reduce-scatter.2
  125.8 24.7 reduce-scatter.4
where the time goes:
time: 160 us
  waiting for transfers between devices  82 us (51%)
  blocking collectives  26.4 us (16%)
  matrix products  14.7 us (9%)
  between operations  13.3 us (8%)
  local copies, waits for them, and re-layouts  12.1 us (8%)
  other arithmetic  6.9 us (4%)
  starting transfers between devices  4.68 us (3%)
    reduce_scatter x1, waiting for transfers between devices, body(): lax.psum_scatter(routed_terms.astype(jnp.bfloat16), 'tp', scatter_dimensi...  34.5 us
    all_gather x1, waiting for transfers between devices, body(): piece = lax.all_gather(arrived, 'tp', axis=2, tiled=True)  27.7 us
    all_to_all x1, blocking collectives, body(): lax.all_to_all(own_columns, 'ep', split_axis=0, concat_axis=0, tiled=True)  26.4 us
    all_to_all x1, waiting for transfers between devices, body(): lax.all_to_all(expert_out, 'ep', split_axis=0, concat_axis=0, tiled=True)  19.8 us
    dot_general x1, matrix products, body(): jnp.dot(hidden, expert_down[local], preferred_element_type=jnp.float32)  7.39 us
    all_to_all x1, starting transfers between devices, body(): lax.all_to_all(expert_out, 'ep', split_axis=0, concat_axis=0, tiled=True)  4.6 us
    gather x1, local copies, waits for them, and re-layouts, body(): outgoing = padded[slot_token].reshape(experts, capacity, width)  4.27 us
    dot_general x1, matrix products, body(): gate_list = [jnp.dot(rows, gate_rows, preferred_element_type=jnp.float32)]  3.76 us
  transfers between devices with their start and end apart: 4, of which 3 were waited for; matrix products, arithmetic and copies ran while one was open for 5% of the time, Pallas kernels for 0%

commit v1 on v0

v1 whole, which is shorter than its diff:
```python
import jax
import jax.numpy as jnp
from jax import lax
from jax.experimental import pallas as pl
from jax.experimental.pallas import tpu as pltpu
from jax.sharding import PartitionSpec as P


BF, F32 = jnp.bfloat16, jnp.float32
VM = pltpu.MemorySpace.VMEM


def norm_rows(tokens, norm_gain):
    values = tokens.astype(jnp.float32)
    scale = lax.rsqrt(jnp.mean(values * values, axis=-1, keepdims=True) + 1e-06)
    return (values * scale * norm_gain).astype(jnp.bfloat16)


def dot(a, b):
    return jnp.dot(a, b, preferred_element_type=F32)


def swiglu(gate, up):
    return (gate / (1.0 + jnp.exp(-gate)) * up).astype(BF)


def call(kernel, outs, args, mib=16, **more):
    return pl.pallas_call(
        kernel,
        out_shape=outs,
        in_specs=[pl.BlockSpec(memory_space=VM)] * len(args),
        out_specs=jax.tree.map(lambda _: pl.BlockSpec(memory_space=VM), outs),
        compiler_params=pltpu.CompilerParams(vmem_limit_bytes=mib * 1024 * 1024),
        **more,
    )(*args)


def places_of(routing, ep, experts, capacity):
    top, rows = routing.shape
    expert = lax.broadcasted_iota(jnp.int32, (max(8, experts), rows), 0)
    hits = [(routing[k : k + 1, :] == expert).astype(F32) for k in range(top)]
    named = sum(hits[1:], hits[0])
    before = lax.broadcasted_iota(jnp.int32, (rows, rows), 0)
    at = lax.broadcasted_iota(jnp.int32, (rows, rows), 1)
    earlier = dot(named.astype(BF), (before < at).astype(F32).astype(BF))
    places = []
    for k in range(top):
        slot = jnp.sum(earlier * hits[k], axis=0, keepdims=True)
        turn = routing[k : k + 1, :] - ep
        turn = jnp.where(turn < 0, turn + experts, turn)
        places.append((turn * capacity).astype(F32) + slot)
    return places


def fast_body(
    tokens, norm_gain, routing, gate_weights, expert_gate, expert_up, expert_down, shared_gate, shared_up, shared_down
):
    ep_count, tp_count = lax.axis_size("ep"), lax.axis_size("tp")
    rows, width = tokens.shape
    top = routing.shape[1]
    experts = ep_count
    capacity = max(2, 3 * rows * top // (2 * experts))
    quarter = width // tp_count
    half = width // 2
    part = capacity // CORES
    w_gate, w_up, w_down = expert_gate[0], expert_up[0], expert_down[0]
    order = shift_order(ep_count)
    routing, gate_weights = routing.T, gate_weights.T

    def over_tp(x, m):
        return lax.ppermute(x, "tp", [(i, i ^ m) for i in range(tp_count)])

    def over_ep(x, s):
        return lax.ppermute(x, "ep", [(i, (i + s) % ep_count) for i in range(ep_count)])

    def at_quarter(m):
        return pl.ds(pl.multiple_of((lax.axis_index("tp") ^ m) * quarter, quarter), quarter)

    def at_half(other):
        chip = lax.axis_index("tp") // CORES
        return pl.ds(pl.multiple_of((1 - chip if other else chip) * half, half), half)

    near_gate, near_up = over_tp(w_gate, 1), over_tp(w_up, 1)
    near_down = over_tp(w_down, 1)

    def dispatch(tokens_ref, gain_ref, routing_ref, normed_ref, *send_refs):
        values = tokens_ref[...].astype(F32)
        scale = lax.rsqrt(jnp.mean(values * values, axis=-1, keepdims=True) + 1e-06)
        normed_ref[...] = (values * scale * gain_ref[...]).astype(BF)
        places = places_of(routing_ref[...], lax.axis_index("ep"), experts, capacity)
        places = [p.astype(jnp.int32) for p in places]
        mine = normed_ref[:, at_half(False)]
        base = (lax.axis_index("tp") % CORES) * part
        for send_ref, s in zip(send_refs, order):
            index = lax.broadcasted_iota(jnp.int32, (part, rows), 0) + (base + s * capacity)
            pick = (index == places[0]).astype(F32)
            for p in places[1:]:
                pick = pick + (index == p).astype(F32)
            send_ref[...] = dot(pick.astype(BF), mine).astype(BF)

    piece = jax.ShapeDtypeStruct((part, half), BF)
    normed, *sends = call(
        dispatch,
        [jax.ShapeDtypeStruct((rows, width), BF)] + [piece] * len(order),
        [tokens, norm_gain.reshape(1, width), routing],
    )
    arrived = [over_ep(x, s) for x, s in zip(sends, order)]

    def local(normed_ref, routing_ref, gw_ref, wg, wu, wd, sg, su, sd, *refs):
        out_refs, info_ref, pick_refs = refs[:tp_count], refs[tp_count], refs[tp_count + 1 :]
        places = places_of(routing_ref[...], lax.axis_index("ep"), experts, capacity)
        index = lax.broadcasted_iota(jnp.int32, (capacity, rows), 0)
        own = (index == places[0].astype(jnp.int32)).astype(F32)
        for p in places[1:]:
            own = own + (index == p.astype(jnp.int32)).astype(F32)
        own_rows = dot(own.astype(BF), normed_ref[...]).astype(BF)
        hidden = swiglu(dot(own_rows, wg[...]), dot(own_rows, wu[...]))
        s_hidden = swiglu(dot(normed_ref[...], sg[...]), dot(normed_ref[...], su[...]))
        info = jnp.zeros((128, rows), F32)
        line = lax.broadcasted_iota(jnp.int32, (128, rows), 0)
        for k in range(top):
            info = jnp.where(line == k, places[k], info)
            info = jnp.where(line == top + k, gw_ref[k : k + 1, :], info)
        info = info.T
        info_ref[...] = info
        lanes = lax.broadcasted_iota(jnp.int32, (rows, capacity), 1)
        columns = [info[:, k : k + 1].astype(jnp.int32) for k in range(top)]
        weights = [info[:, top + k : top + k + 1] for k in range(top)]
        pick = (columns[0] == lanes).astype(F32)
        weight = jnp.where(columns[0] < capacity, weights[0], 0.0)
        for k in range(1, top):
            pick = pick + (columns[k] == lanes).astype(F32)
            weight = weight + jnp.where(columns[k] < capacity, weights[k], 0.0)
        pick = pick.astype(BF)
        for m in range(tp_count):
            term = dot(hidden, wd[:, at_quarter(m)]).astype(BF)
            shared = dot(s_hidden, sd[:, at_quarter(m)])
            out_refs[m][...] = (dot(pick, term) * weight + shared).astype(BF)
        lanes = lax.broadcasted_iota(jnp.int32, (rows, part), 1)
        base = (lax.axis_index("tp") % CORES) * part
        for i, s in enumerate(order):
            for k in range(top):
                pick_refs[i * top + k][...] = (columns[k] == lanes + (base + s * capacity)).astype(F32).astype(BF)

    out_piece = jax.ShapeDtypeStruct((rows, quarter), BF)
    partials = call(
        local,
        [out_piece] * tp_count
        + [jax.ShapeDtypeStruct((rows, 128), F32)]
        + [jax.ShapeDtypeStruct((rows, part), BF)] * (top * len(order)),
        [normed, routing, gate_weights, w_gate, w_up, w_down, shared_gate, shared_up, shared_down],
    )
    info, picks = partials[tp_count], partials[tp_count + 1 :]
    partials = partials[:tp_count]

    def add(*refs):
        n = len(refs) // 3
        for i in range(n):
            refs[2 * n + i][...] = (refs[i][...].astype(F32) + refs[n + i][...].astype(F32)).astype(BF)

    keep = [m for m in range(tp_count) if m % CORES == 0]
    came = [over_tp(partials[m ^ 1], 1) for m in keep]
    sums = call(add, [out_piece] * len(keep), [partials[m] for m in keep] + came)
    kept = [sums[0], over_tp(sums[1], CORES)]

    def expert(*refs):
        mine_ref, came_ref, ws, outs = refs[0], refs[1], refs[2:8], refs[8:]
        total = [None, None]
        for wg, wu, wd in (ws[0:3], ws[3:6]):
            gate = dot(mine_ref[...], wg[at_half(False), :]) + dot(came_ref[...], wg[at_half(True), :])
            up = dot(mine_ref[...], wu[at_half(False), :]) + dot(came_ref[...], wu[at_half(True), :])
            hidden = swiglu(gate, up)
            for i in range(2):
                term = dot(hidden, wd[:, at_half(i == 1)])
                total[i] = term if total[i] is None else total[i] + term
        for i in range(2):
            outs[i][...] = total[i].astype(BF)

    returned = []
    for x, s in zip(arrived, order):
        came = over_tp(x, CORES)
        mine, other = call(expert, [piece] * 2, [x, came, w_gate, w_up, w_down, near_gate, near_up, near_down])
        more = over_tp(other, CORES)
        (out,) = call(add, [piece], [mine, more])
        returned.append(over_ep(out, ep_count - s))

    def combine(info_ref, *refs):
        chosen, back, sofar, outs = refs[:top], refs[top], refs[top + 1 : -2], refs[-2:]
        core = lax.axis_index("tp") % CORES
        for i in range(2):
            at = pl.ds(pl.multiple_of((core if i == 0 else 1 - core) * quarter, quarter), quarter)
            total = sofar[i][...].astype(F32) if sofar else jnp.zeros((rows, quarter), F32)
            for k in range(top):
                total = total + dot(chosen[k][...], back[:, at]) * info_ref[:, top + k : top + k + 1]
            outs[i][...] = total.astype(outs[i].dtype)

    sofar = []
    wide = jax.ShapeDtypeStruct((rows, quarter), F32)
    for i, (back, s) in enumerate(zip(returned, order)):
        kind = [wide, out_piece if i + 1 == len(order) else wide]
        sofar = call(combine, kind, [info, *picks[i * top : i * top + top], back, *sofar])

    def finish(mine_ref, more_ref, near_ref, far_ref, out_ref):
        total = mine_ref[...] + more_ref[...].astype(F32)
        out_ref[...] = (total + near_ref[...].astype(F32) + far_ref[...].astype(F32)).astype(BF)

    return call(finish, out_piece, [sofar[0], over_tp(sofar[1], 1), *kept])


CORES = 2


def shift_order(ep_count):
    return list(range(1, ep_count))


def general_body(
    tokens, norm_gain, routing, gate_weights, expert_gate, expert_up, expert_down, shared_gate, shared_up, shared_down
):
    ep_count = lax.axis_size("ep")
    tp_count = lax.axis_size("tp")
    tok_rows, width = tokens.shape
    top = routing.shape[1]
    local_experts = expert_gate.shape[0]
    experts = ep_count * local_experts
    capacity = max(2, 3 * tok_rows * top // (2 * experts))
    quarter = width // tp_count
    arrived_rows = ep_count * capacity
    normed = norm_rows(tokens, norm_gain)
    flat_experts = routing.reshape(-1)
    assign = flat_experts.shape[0]
    onehot = (flat_experts[:, None] == jnp.arange(experts, dtype=jnp.int32)[None, :]).astype(jnp.float32)
    lower = (jnp.arange(assign)[:, None] >= jnp.arange(assign)[None, :]).astype(jnp.float32)
    running = jnp.dot(lower, onehot, precision=lax.Precision.HIGHEST)
    slot = (jnp.sum(running * onehot, axis=1) - 1.0).astype(jnp.int32)
    dest = flat_experts * capacity + slot
    owner = jnp.arange(assign, dtype=jnp.int32) // top
    slot_token = jnp.full((experts * capacity,), tok_rows, jnp.int32).at[dest].set(owner)
    padded = jnp.concatenate([normed, jnp.zeros((1, width), jnp.bfloat16)], axis=0)
    outgoing = padded[slot_token].reshape(experts, capacity, width)
    position = lax.axis_index("tp")
    own_columns = lax.dynamic_slice_in_dim(outgoing, position * quarter, quarter, 2)
    arrived = lax.all_to_all(own_columns, "ep", split_axis=0, concat_axis=0, tiled=True)
    piece = lax.all_gather(arrived, "tp", axis=2, tiled=True)
    piece = piece.reshape(ep_count, local_experts, capacity, width)
    routed_list = []
    for local in range(local_experts):
        rows = piece[:, local].reshape(arrived_rows, width)
        gate = jnp.dot(rows, expert_gate[local], preferred_element_type=jnp.float32)
        up = jnp.dot(rows, expert_up[local], preferred_element_type=jnp.float32)
        hidden = (jax.nn.silu(gate) * up).astype(jnp.bfloat16)
        term = jnp.dot(hidden, expert_down[local], preferred_element_type=jnp.float32)
        routed_list.append(term.reshape(ep_count, capacity, width))
    routed_terms = jnp.stack(routed_list, axis=1).reshape(experts * capacity, width)
    shared_gate_rows = jnp.dot(normed, shared_gate, preferred_element_type=jnp.float32)
    shared_up_rows = jnp.dot(normed, shared_up, preferred_element_type=jnp.float32)
    shared_hidden = (jax.nn.silu(shared_gate_rows) * shared_up_rows).astype(jnp.bfloat16)
    shared_term = jnp.dot(shared_hidden, shared_down, preferred_element_type=jnp.float32)
    routed_sum, shared_sum = (
        lax.psum_scatter(x.astype(jnp.bfloat16), "tp", scatter_dimension=1, tiled=True).astype(jnp.float32)
        for x in (routed_terms, shared_term)
    )
    expert_out = routed_sum.astype(jnp.bfloat16).reshape(experts, capacity, quarter)
    returned = lax.all_to_all(expert_out, "ep", split_axis=0, concat_axis=0, tiled=True)
    picked = returned.reshape(experts * capacity, quarter)[dest]
    picked = picked.astype(jnp.float32).reshape(tok_rows, top, quarter)
    routed = jnp.sum(picked * gate_weights[:, :, None], axis=1)
    return (routed + shared_sum).astype(jnp.bfloat16)


def solution(mesh):
    in_specs = (
        P(("grp", "ep"), None),
        P(),
        P(("grp", "ep"), None),
        P(("grp", "ep"), None),
        P("ep", None, "tp"),
        P("ep", None, "tp"),
        P("ep", "tp", None),
        P(None, "tp"),
        P(None, "tp"),
        P("tp", None),
    )
    ep_count, tp_count = mesh.shape["ep"], mesh.shape["tp"]

    def step(body):
        return jax.shard_map(body, mesh=mesh, in_specs=in_specs, out_specs=P(("grp", "ep"), "tp"), check_vma=False)

    if ep_count <= 2 * tp_count and tp_count == 2 * CORES:
        return step(fast_body)
    return step(general_body)
```

time: 160 us -> 67.8 us (0.42)
  waiting for transfers between devices: 82 us -> 32.5 us
  blocking collectives: 26.4 us -> 0 us
  starting transfers between devices: 4.68 us -> 20 us
  matrix products: 14.7 us -> 0 us
  between operations: 13.3 us -> 0.25 us
  Pallas kernels: 0 us -> 9.67 us
  local copies, waits for them, and re-layouts: 12.1 us -> 5.09 us
  other arithmetic: 6.9 us -> 0 us
    reduce_scatter x2 -> x0, waiting for transfers between devices: 34.5 us -> none  [the longest x1 34.5 us: body(): lax.psum_scatter(routed_terms.astype(jnp.bfloat16), 'tp', scatter_dimensi...]
    ppermute x0 -> x19, waiting for transfers between devices: none -> 32.5 us  [the longest x6 26 us: over_ep(): lax.ppermute(x, 'ep', [(i, (i + s) % ep_count) for i in range(ep_count)])]
    all_gather x1 -> x0, waiting for transfers between devices: 27.7 us -> none  [body(): piece = lax.all_gather(arrived, 'tp', axis=2, tiled=True)]
    all_to_all x1 -> x0, blocking collectives: 26.4 us -> none  [body(): lax.all_to_all(own_columns, 'ep', split_axis=0, concat_axis=0, tiled=True)]
    ppermute x0 -> x19, starting transfers between devices: none -> 20 us  [the longest x13 11.4 us: over_tp(): return lax.ppermute(x, 'tp', [(i, i ^ m) for i in range(tp_count)])]
    all_to_all x1 -> x0, waiting for transfers between devices: 19.8 us -> none  [body(): lax.all_to_all(expert_out, 'ep', split_axis=0, concat_axis=0, tiled=True)]
    dot_general x5 -> x0, matrix products: 14.7 us -> none  [the longest x1 7.39 us: body(): jnp.dot(hidden, expert_down[local], preferred_element_type=jnp.float32)]
    pallas_call x0 -> x13, Pallas kernels: none -> 9.67 us  [call(): pl.pallas_call(kernel, out_shape=outs, in_specs=[pl.BlockSpec(memory_spac...]
  transfers between devices with their start and end apart: 4 -> 19, of which waited for: 3 -> 9; matrix products, arithmetic and copies ran while one was open for 5% -> 0% of each run, Pallas kernels for 0% -> 13%
where the time goes in v1:
time: 67.8 us; the launch traced here: 67.5 us
  waiting for transfers between devices  32.5 us (48%)
  starting transfers between devices  20 us (29%)
  Pallas kernels  9.67 us (14%)
  local copies, waits for them, and re-layouts  5.09 us (8%)
    ppermute x6, waiting for transfers between devices, over_ep(): lax.ppermute(x, 'ep', [(i, (i + s) % ep_count) for i in range(ep_count)])  26 us
    ppermute x13, starting transfers between devices, over_tp(): return lax.ppermute(x, 'tp', [(i, i ^ m) for i in range(tp_count)])  11.4 us
    pallas_call x13, Pallas kernels, call(): pl.pallas_call(kernel, out_shape=outs, in_specs=[pl.BlockSpec(memory_spac...  9.67 us
    ppermute x6, starting transfers between devices, over_ep(): lax.ppermute(x, 'ep', [(i, (i + s) % ep_count) for i in range(ep_count)])  8.59 us
    ppermute x13, waiting for transfers between devices, over_tp(): return lax.ppermute(x, 'tp', [(i, i ^ m) for i in range(tp_count)])  6.53 us
    unnamed x26, local copies, waits for them, and re-layouts  5.09 us
  transfers between devices with their start and end apart: 19, of which 9 were waited for; matrix products, arithmetic and copies ran while one was open for 0% of the time, Pallas kernels for 13%

profile of v1, /device:TPU:0, one launch (start us, length us, event | category | flops | bytes accessed | tf_op | source)
XLA Modules:
  0.0 67.5 jit_solution(15688339955465911092)
XLA Ops:
  0.0 0.5 collective-permute-start.2
  0.5 0.1 collective-permute-start.3
  0.6 0.4 collective-permute-start.4
  1.0 1.2 %copy-done.5 = bf16[256,2048]{1,0:T(8,128)(2,1)S(1)} copy-done((bf16[256,2048]{1,0:T(8,128)(2,1)S(1)}, bf16[256,2048]{1,0:T(8,128)(2,1)}, u32[]{:S(2)}) %copy-start.5) | copy-done | bytes 1048600
  2.2 0.7 %copy-done.9 = s32[256,2]{0,1:T(2,128)S(1)} copy-done((s32[256,2]{0,1:T(2,128)S(1)}, s32[256,2]{0,1:T(2,128)}, u32[]{:S(2)}) %copy-start.9) | copy-done | bytes 2072
  2.9 0.7 %copy-done.11 = f32[2048]{0:T(1024)S(1)} copy-done((f32[2048]{0:T(1024)S(1)}, f32[2048]{0:T(1024)}, u32[]{:S(2)}) %copy-start.11) | copy-done | bytes 8216
  3.6 1.0 %shard_map.100 = (bf16[256,2048]{1,0:T(8,128)(2,1)S(1)}, bf16[96,1024]{1,0:T(8,128)(2,1)S(1)}, bf16[96,1024]{1,0:T(8,128)(2,1)S(1)}, bf16[96,1024]{1,0:T(8,128)(2,1)S(1)}) custom-call(bf16[256,2048]{1,0:T(8,128)(2,1)S(1)} %copy-done.5, f32[1,2048]{1,0:T(1,128)S(1)} %bitcast.23, s32[2,256]{1,0:T(2,128)S(1)} %bitcast.21), custom_call_target="tpu_custom_call" | custom-call | tf_op jit(solution)/shard_map/pallas_call | solution.py:28
  4.6 4.7 %collective-permute-start = (bf16[96,1024]{1,0:T(8,128)(2,1)S(1)}, bf16[96,1024]{1,0:T(8,128)(2,1)S(1)}, u32[]{:S(2)}, u32[]{:S(2)}) collective-permute-start(bf16[96,1024]{1,0:T(8,128)(2,1)S(1)} %get-tuple-element.38), channel_id=1, source_target_pairs={{0,12},{4,0},{8,4},{12,8},{1,13},{5,1},{9,5},{13,9},{2,14},{6,2},{... | collective-permute-start | bytes 589832 | tf_op jit(solution)/shard_map/ppermute | solution.py:74
  9.3 5.3 %collective-permute-done.refs_0_ = bf16[96,1024]{1,0:T(8,128)(2,1)S(1)} collective-permute-done((bf16[96,1024]{1,0:T(8,128)(2,1)S(1)}, bf16[96,1024]{1,0:T(8,128)(2,1)S(1)}, u32[]{:S(2)}, u32[]{:S(2)}) %collective-permute-start) | collective-permute-done | bytes 196640 | tf_op jit(solution)/shard_map/ppermute | solution.py:74
  14.7 1.4 %collective-permute-start.7 = (bf16[96,1024]{1,0:T(8,128)(2,1)S(1)}, bf16[96,1024]{1,0:T(8,128)(2,1)S(1)}, u32[]{:S(2)}, u32[]{:S(2)}) collective-permute-start(bf16[96,1024]{1,0:T(8,128)(2,1)S(1)} %get-tuple-element.43), channel_id=1, source_target_pairs={{0,8},{4,12},{8,0},{12,4},{1,9},{5,13},{9,1},{13,5},{2,10},{6,14},... | collective-permute-start | bytes 589832 | tf_op jit(solution)/shard_map/ppermute | solution.py:74
  16.1 3.6 %collective-permute-done.11.refs_0_ = bf16[96,1024]{1,0:T(8,128)(2,1)S(1)} collective-permute-done((bf16[96,1024]{1,0:T(8,128)(2,1)S(1)}, bf16[96,1024]{1,0:T(8,128)(2,1)S(1)}, u32[]{:S(2)}, u32[]{:S(2)}) %collective-permute-start.11) | collective-permute-done | bytes 196640 | tf_op jit(solution)/shard_map/ppermute | solution.py:74
  19.7 1.5 %collective-permute-start.12 = (bf16[96,1024]{1,0:T(8,128)(2,1)S(1)}, bf16[96,1024]{1,0:T(8,128)(2,1)S(1)}, u32[]{:S(2)}, u32[]{:S(2)}) collective-permute-start(bf16[96,1024]{1,0:T(8,128)(2,1)S(1)} %collective-permute-done.11.refs_0_), channel_id=1, source_target_pairs={{0,2},{1,3},{2,0},{3,1},{4,6},{5,7},{6,4},{7,5},{8,10},{9,11},{10,... | collective-permute-start | bytes 589832 | tf_op jit(solution)/shard_map/ppermute | solution.py:71
  21.2 6.5 %collective-permute-done.7.refs_0_ = bf16[96,1024]{1,0:T(8,128)(2,1)S(1)} collective-permute-done((bf16[96,1024]{1,0:T(8,128)(2,1)S(1)}, bf16[96,1024]{1,0:T(8,128)(2,1)S(1)}, u32[]{:S(2)}, u32[]{:S(2)}) %collective-permute-start.7) | collective-permute-done | bytes 196640 | tf_op jit(solution)/shard_map/ppermute | solution.py:74
  27.6 1.5 %collective-permute-start.8 = (bf16[96,1024]{1,0:T(8,128)(2,1)S(1)}, bf16[96,1024]{1,0:T(8,128)(2,1)S(1)}, u32[]{:S(2)}, u32[]{:S(2)}) collective-permute-start(bf16[96,1024]{1,0:T(8,128)(2,1)S(1)} %collective-permute-done.7.refs_0_), channel_id=1, source_target_pairs={{0,2},{1,3},{2,0},{3,1},{4,6},{5,7},{6,4},{7,5},{8,10},{9,11},{10,... | collective-permute-start | bytes 589832 | tf_op jit(solution)/shard_map/ppermute | solution.py:71
  29.1 0.5 collective-permute-start.1
  29.7 0.0 copy-start.1
  29.7 1.2 %copy-done.1 = bf16[1,2048,256]{2,1,0:T(8,128)(2,1)S(1)} copy-done((bf16[1,2048,256]{2,1,0:T(8,128)(2,1)S(1)}, bf16[1,2048,256]{2,1,0:T(8,128)(2,1)}, u32[]{:S(2)}) %copy-start.1) | copy-done | bytes 1048600
  30.9 1.2 %copy-done.3 = bf16[1,256,2048]{2,1,0:T(8,128)(2,1)S(1)} copy-done((bf16[1,256,2048]{2,1,0:T(8,128)(2,1)S(1)}, bf16[1,256,2048]{2,1,0:T(8,128)(2,1)}, u32[]{:S(2)}) %copy-start.3) | copy-done | bytes 1048600
  32.1 1.2 %shard_map.106 = (bf16[96,1024]{1,0:T(8,128)(2,1)S(1)}, bf16[96,1024]{1,0:T(8,128)(2,1)S(1)}) custom-call(bf16[96,1024]{1,0:T(8,128)(2,1)S(1)} %collective-permute-done.11.refs_0_, bf16[96,1024]{1,0:T(8,128)(2,1)S(1)} %collective-permute-done.12.refs_1_, bf16[2048,256]{1,0:T(8,128)(2,1)S(1)} %bitcast.7, bf16[2048,256]{1,0:T(8,128)(2,1)S(1)} %bitcast.12, ...), custom_call_target="tpu_custom_call" | custom-call | tf_op jit(solution)/shard_map/pallas_call | solution.py:28
  33.4 1.6 %collective-permute-start.13 = (bf16[96,1024]{1,0:T(8,128)(2,1)S(1)}, bf16[96,1024]{1,0:T(8,128)(2,1)S(1)}, u32[]{:S(2)}, u32[]{:S(2)}) collective-permute-start(bf16[96,1024]{1,0:T(8,128)(2,1)S(1)} %get-tuple-element.50), channel_id=1, source_target_pairs={{0,2},{1,3},{2,0},{3,1},{4,6},{5,7},{6,4},{7,5},{8,10},{9,11},{10,... | collective-permute-start | bytes 589832 | tf_op jit(solution)/shard_map/ppermute | solution.py:71
  34.9 0.5 collective-permute-done.8.refs_1_
  35.4 1.2 %shard_map.104 = (bf16[96,1024]{1,0:T(8,128)(2,1)S(1)}, bf16[96,1024]{1,0:T(8,128)(2,1)S(1)}) custom-call(bf16[96,1024]{1,0:T(8,128)(2,1)S(1)} %collective-permute-done.7.refs_0_, bf16[96,1024]{1,0:T(8,128)(2,1)S(1)} %collective-permute-done.8.refs_1_, bf16[2048,256]{1,0:T(8,128)(2,1)S(1)} %bitcast.8, bf16[2048,256]{1,0:T(8,128)(2,1)S(1)} %bitcast.13, ...), custom_call_target="tpu_custom_call" | custom-call | tf_op jit(solution)/shard_map/pallas_call | solution.py:28
  36.6 0.0 copy-start.2
  36.7 0.0 copy-start.4
  36.7 0.0 copy-start.7
  36.7 0.0 copy-start.8
  36.7 1.6 %collective-permute-start.9 = (bf16[96,1024]{1,0:T(8,128)(2,1)S(1)}, bf16[96,1024]{1,0:T(8,128)(2,1)S(1)}, u32[]{:S(2)}, u32[]{:S(2)}) collective-permute-start(bf16[96,1024]{1,0:T(8,128)(2,1)S(1)} %get-tuple-element.45), channel_id=1, source_target_pairs={{0,2},{1,3},{2,0},{3,1},{4,6},{5,7},{6,4},{7,5},{8,10},{9,11},{10,... | collective-permute-start | bytes 589832 | tf_op jit(solution)/shard_map/ppermute | solution.py:71
  38.3 1.3 %collective-permute-done.1.refs_1_ = bf16[96,1024]{1,0:T(8,128)(2,1)S(1)} collective-permute-done((bf16[96,1024]{1,0:T(8,128)(2,1)S(1)}, bf16[96,1024]{1,0:T(8,128)(2,1)S(1)}, u32[]{:S(2)}, u32[]{:S(2)}) %collective-permute-start.1) | collective-permute-done | bytes 196640 | tf_op jit(solution)/shard_map/ppermute | solution.py:71
  39.6 1.2 %shard_map.102 = (bf16[96,1024]{1,0:T(8,128)(2,1)S(1)}, bf16[96,1024]{1,0:T(8,128)(2,1)S(1)}) custom-call(bf16[96,1024]{1,0:T(8,128)(2,1)S(1)} %collective-permute-done.refs_0_, bf16[96,1024]{1,0:T(8,128)(2,1)S(1)} %collective-permute-done.1.refs_1_, bf16[2048,256]{1,0:T(8,128)(2,1)S(1)} %bitcast.9, bf16[2048,256]{1,0:T(8,128)(2,1)S(1)} %bitcast.14, ...), custom_call_target="tpu_custom_call" | custom-call | tf_op jit(solution)/shard_map/pallas_call | solution.py:28
  40.9 1.6 %collective-permute-start.5 = (bf16[96,1024]{1,0:T(8,128)(2,1)S(1)}, bf16[96,1024]{1,0:T(8,128)(2,1)S(1)}, u32[]{:S(2)}, u32[]{:S(2)}) collective-permute-start(bf16[96,1024]{1,0:T(8,128)(2,1)S(1)} %get-tuple-element.40), channel_id=1, source_target_pairs={{0,2},{1,3},{2,0},{3,1},{4,6},{5,7},{6,4},{7,5},{8,10},{9,11},{10,... | collective-permute-start | bytes 589832 | tf_op jit(solution)/shard_map/ppermute | solution.py:71
  42.5 2.5 %shard_map.101 = (bf16[256,512]{1,0:T(8,128)(2,1)S(1)}, bf16[256,512]{1,0:T(8,128)(2,1)S(1)}, bf16[256,512]{1,0:T(8,128)(2,1)S(1)}, bf16[256,512]{1,0:T(8,128)(2...) custom-call(bf16[256,2048]{1,0:T(8,128)(2,1)S(1)} %get-tuple-element, ...), custom_call_target="tpu_custom_call" | custom-call | tf_op jit(solution)/shard_map/pallas_call | solution.py:28
  45.0 0.1 collective-permute-start.16
  45.1 0.5 collective-permute-start.17
  45.6 2.3 %collective-permute-start.14 = (bf16[96,1024]{1,0:T(8,128)(2,1)S(1)}, bf16[96,1024]{1,0:T(8,128)(2,1)S(1)}, u32[]{:S(2)}, u32[]{:S(2)}) collective-permute-start(bf16[96,1024]{1,0:T(8,128)(2,1)S(1)} %shard_map.107), channel_id=1, source_target_pairs={{0,12},{4,0},{8,4},{12,8},{1,13},{5,1},{9,5},{13,9},{2,14},{6,2},{... | collective-permute-start | bytes 589832 | tf_op jit(solution)/shard_map/ppermute | solution.py:74
  48.0 0.1 collective-permute-done.9.refs_1_
  48.1 0.1 collective-permute-start.10
  48.2 3.1 %collective-permute-done.5.refs_1_ = bf16[96,1024]{1,0:T(8,128)(2,1)S(1)} collective-permute-done((bf16[96,1024]{1,0:T(8,128)(2,1)S(1)}, bf16[96,1024]{1,0:T(8,128)(2,1)S(1)}, u32[]{:S(2)}, u32[]{:S(2)}) %collective-permute-start.5) | collective-permute-done | bytes 196640 | tf_op jit(solution)/shard_map/ppermute | solution.py:71
  51.4 0.1 collective-permute-start.6
  51.4 0.1 shard_map.111
  51.6 1.6 %collective-permute-start.18 = (bf16[256,512]{1,0:T(8,128)(2,1)S(1)}, bf16[256,512]{1,0:T(8,128)(2,1)S(1)}, u32[]{:S(2)}, u32[]{:S(2)}) collective-permute-start(bf16[256,512]{1,0:T(8,128)(2,1)S(1)} %get-tuple-element.62), channel_id=1, source_target_pairs={{0,2},{1,3},{2,0},{3,1},{4,6},{5,7},{6,4},{7,5},{8,10},{9,11},{10,... | collective-permute-start | bytes 786440 | tf_op jit(solution)/shard_map/ppermute | solution.py:71
  53.1 1.1 %collective-permute-done.14.refs_2_ = bf16[96,1024]{1,0:T(8,128)(2,1)S(1)} collective-permute-done((bf16[96,1024]{1,0:T(8,128)(2,1)S(1)}, bf16[96,1024]{1,0:T(8,128)(2,1)S(1)}, u32[]{:S(2)}, u32[]{:S(2)}) %collective-permute-start.14) | collective-permute-done | bytes 196640 | tf_op jit(solution)/shard_map/ppermute | solution.py:74
  54.2 0.4 shard_map.108
  54.7 9.5 %collective-permute-done.10.refs_2_ = bf16[96,1024]{1,0:T(8,128)(2,1)S(1)} collective-permute-done((bf16[96,1024]{1,0:T(8,128)(2,1)S(1)}, bf16[96,1024]{1,0:T(8,128)(2,1)S(1)}, u32[]{:S(2)}, u32[]{:S(2)}) %collective-permute-start.10) | collective-permute-done | bytes 196640 | tf_op jit(solution)/shard_map/ppermute | solution.py:74
  64.1 0.5 shard_map.109
  64.6 0.5 shard_map.110
  65.1 0.1 collective-permute-start.15
  65.2 1.5 %collective-permute-done.15.more_ref = bf16[256,512]{1,0:T(8,128)(2,1)S(1)} collective-permute-done((bf16[256,512]{1,0:T(8,128)(2,1)S(1)}, bf16[256,512]{1,0:T(8,128)(2,1)S(1)}, u32[]{:S(2)}, u32[]{:S(2)}) %collective-permute-start.15) | collective-permute-done | bytes 262176 | tf_op jit(solution)/shard_map/ppermute | solution.py:71
  66.7 0.8 %shard_map.112 = bf16[256,512]{1,0:T(8,128)(2,1)} custom-call(f32[256,512]{1,0:T(8,128)S(1)} %get-tuple-element.55.mine_ref, bf16[256,512]{1,0:T(8,128)(2,1)S(1)} %collective-permute-done.15.more_ref, bf16[256,512]{1,0:T(8,128)(2,1)S(1)} %get-tuple-element.61.near_ref, bf16[256,512]{1,0:T(8,128)(2,1)S(1)} %collective-permute-done.18.far_ref), custom_call_target="tpu_custom_call" | custom-call | tf_op jit(solution)/shard_map/pallas_call | solution.py:28
  (29 shorter events, 0.2 us)
Async XLA Ops:
  0.0 29.7 %copy-start = (bf16[1,2048,256]{2,1,0:T(8,128)(2,1)S(1)}, bf16[1,2048,256]{2,1,0:T(8,128)(2,1)}, u32[]{:S(2)}) copy-start(bf16[1,2048,256]{2,1,0:T(8,128)(2,1)} %param.14) | copy-start | bytes 3145732
  0.0 29.7 %collective-permute-start.2 = (bf16[2048,256]{1,0:T(8,128)(2,1)}, bf16[2048,256]{1,0:T(8,128)(2,1)S(1)}, u32[]{:S(2)}, u32[]{:S(2)}) collective-permute-start(bf16[2048,256]{1,0:T(8,128)(2,1)} %bitcast.6), channel_id=1, source_target_pairs={{0,1},{1,0},{2,3},{3,2},{4,5},{5,4},{6,7},{7,6},{8,9},{9,8},{10,11... | collective-permute-start | bytes 3145736 | tf_op jit(solution)/shard_map/ppermute | solution.py:71
  0.5 29.2 %collective-permute-start.3 = (bf16[2048,256]{1,0:T(8,128)(2,1)}, bf16[2048,256]{1,0:T(8,128)(2,1)S(1)}, u32[]{:S(2)}, u32[]{:S(2)}) collective-permute-start(bf16[2048,256]{1,0:T(8,128)(2,1)} %bitcast.11), channel_id=1, source_target_pairs={{0,1},{1,0},{2,3},{3,2},{4,5},{5,4},{6,7},{7,6},{8,9},{9,8},{10,11... | collective-permute-start | bytes 3145736 | tf_op jit(solution)/shard_map/ppermute | solution.py:71
  0.6 29.1 %collective-permute-start.4 = (bf16[256,2048]{1,0:T(8,128)(2,1)}, bf16[256,2048]{1,0:T(8,128)(2,1)S(1)}, u32[]{:S(2)}, u32[]{:S(2)}) collective-permute-start(bf16[256,2048]{1,0:T(8,128)(2,1)} %bitcast.16), channel_id=1, source_target_pairs={{0,1},{1,0},{2,3},{3,2},{4,5},{5,4},{6,7},{7,6},{8,9},{9,8},{10,11... | collective-permute-start | bytes 3145736 | tf_op jit(solution)/shard_map/ppermute | solution.py:71
  1.0 1.2 %copy-start.5 = (bf16[256,2048]{1,0:T(8,128)(2,1)S(1)}, bf16[256,2048]{1,0:T(8,128)(2,1)}, u32[]{:S(2)}) copy-start(bf16[256,2048]{1,0:T(8,128)(2,1)} %tokens_ref.1) | copy-start | bytes 3145732
  2.2 0.7 %copy-start.9 = (s32[256,2]{0,1:T(2,128)S(1)}, s32[256,2]{0,1:T(2,128)}, u32[]{:S(2)}) copy-start(s32[256,2]{0,1:T(2,128)} %param.12) | copy-start | bytes 6148
  2.9 0.7 %copy-start.11 = (f32[2048]{0:T(1024)S(1)}, f32[2048]{0:T(1024)}, u32[]{:S(2)}) copy-start(f32[2048]{0:T(1024)} %param.11) | copy-start | bytes 24580
  4.6 10.0 %collective-permute-start = (bf16[96,1024]{1,0:T(8,128)(2,1)S(1)}, bf16[96,1024]{1,0:T(8,128)(2,1)S(1)}, u32[]{:S(2)}, u32[]{:S(2)}) collective-permute-start(bf16[96,1024]{1,0:T(8,128)(2,1)S(1)} %get-tuple-element.38), channel_id=1, source_target_pairs={{0,12},{4,0},{8,4},{12,8},{1,13},{5,1},{9,5},{13,9},{2,14},{6,2},{... | collective-permute-start | bytes 589832 | tf_op jit(solution)/shard_map/ppermute | solution.py:74
  9.3 10.4 %collective-permute-start.11 = (bf16[96,1024]{1,0:T(8,128)(2,1)S(1)}, bf16[96,1024]{1,0:T(8,128)(2,1)S(1)}, u32[]{:S(2)}, u32[]{:S(2)}) collective-permute-start(bf16[96,1024]{1,0:T(8,128)(2,1)S(1)} %get-tuple-element.48), channel_id=1, source_target_pairs={{0,4},{4,8},{8,12},{12,0},{1,5},{5,9},{9,13},{13,1},{2,6},{6,10},{... | collective-permute-start | bytes 589832 | tf_op jit(solution)/shard_map/ppermute | solution.py:74
  14.7 13.0 %collective-permute-start.7 = (bf16[96,1024]{1,0:T(8,128)(2,1)S(1)}, bf16[96,1024]{1,0:T(8,128)(2,1)S(1)}, u32[]{:S(2)}, u32[]{:S(2)}) collective-permute-start(bf16[96,1024]{1,0:T(8,128)(2,1)S(1)} %get-tuple-element.43), channel_id=1, source_target_pairs={{0,8},{4,12},{8,0},{12,4},{1,9},{5,13},{9,1},{13,5},{2,10},{6,14},... | collective-permute-start | bytes 589832 | tf_op jit(solution)/shard_map/ppermute | solution.py:74
  19.7 9.5 %collective-permute-start.12 = (bf16[96,1024]{1,0:T(8,128)(2,1)S(1)}, bf16[96,1024]{1,0:T(8,128)(2,1)S(1)}, u32[]{:S(2)}, u32[]{:S(2)}) collective-permute-start(bf16[96,1024]{1,0:T(8,128)(2,1)S(1)} %collective-permute-done.11.refs_0_), channel_id=1, source_target_pairs={{0,2},{1,3},{2,0},{3,1},{4,6},{5,7},{6,4},{7,5},{8,10},{9,11},{10,... | collective-permute-start | bytes 589832 | tf_op jit(solution)/shard_map/ppermute | solution.py:71
  27.6 7.8 %collective-permute-start.8 = (bf16[96,1024]{1,0:T(8,128)(2,1)S(1)}, bf16[96,1024]{1,0:T(8,128)(2,1)S(1)}, u32[]{:S(2)}, u32[]{:S(2)}) collective-permute-start(bf16[96,1024]{1,0:T(8,128)(2,1)S(1)} %collective-permute-done.7.refs_0_), channel_id=1, source_target_pairs={{0,2},{1,3},{2,0},{3,1},{4,6},{5,7},{6,4},{7,5},{8,10},{9,11},{10,... | collective-permute-start | bytes 589832 | tf_op jit(solution)/shard_map/ppermute | solution.py:71
  29.1 10.5 %collective-permute-start.1 = (bf16[96,1024]{1,0:T(8,128)(2,1)S(1)}, bf16[96,1024]{1,0:T(8,128)(2,1)S(1)}, u32[]{:S(2)}, u32[]{:S(2)}) collective-permute-start(bf16[96,1024]{1,0:T(8,128)(2,1)S(1)} %collective-permute-done.refs_0_), channel_id=1, source_target_pairs={{0,2},{1,3},{2,0},{3,1},{4,6},{5,7},{6,4},{7,5},{8,10},{9,11},{10,... | collective-permute-start | bytes 589832 | tf_op jit(solution)/shard_map/ppermute | solution.py:71
  29.7 1.2 %copy-start.1 = (bf16[1,2048,256]{2,1,0:T(8,128)(2,1)S(1)}, bf16[1,2048,256]{2,1,0:T(8,128)(2,1)}, u32[]{:S(2)}) copy-start(bf16[1,2048,256]{2,1,0:T(8,128)(2,1)} %param.15) | copy-start | bytes 3145732
  30.9 1.2 %copy-start.3 = (bf16[1,256,2048]{2,1,0:T(8,128)(2,1)S(1)}, bf16[1,256,2048]{2,1,0:T(8,128)(2,1)}, u32[]{:S(2)}) copy-start(bf16[1,256,2048]{2,1,0:T(8,128)(2,1)} %param.16) | copy-start | bytes 3145732
  33.4 12.2 %collective-permute-start.13 = (bf16[96,1024]{1,0:T(8,128)(2,1)S(1)}, bf16[96,1024]{1,0:T(8,128)(2,1)S(1)}, u32[]{:S(2)}, u32[]{:S(2)}) collective-permute-start(bf16[96,1024]{1,0:T(8,128)(2,1)S(1)} %get-tuple-element.50), channel_id=1, source_target_pairs={{0,2},{1,3},{2,0},{3,1},{4,6},{5,7},{6,4},{7,5},{8,10},{9,11},{10,... | collective-permute-start | bytes 589832 | tf_op jit(solution)/shard_map/ppermute | solution.py:71
  36.6 5.8 %copy-start.2 = (bf16[1,2048,256]{2,1,0:T(8,128)(2,1)S(1)}, bf16[1,2048,256]{2,1,0:T(8,128)(2,1)}, u32[]{:S(2)}) copy-start(bf16[1,2048,256]{2,1,0:T(8,128)(2,1)} %param.15) | copy-start | bytes 3145732
  36.7 5.8 %copy-start.4 = (bf16[1,256,2048]{2,1,0:T(8,128)(2,1)S(1)}, bf16[1,256,2048]{2,1,0:T(8,128)(2,1)}, u32[]{:S(2)}) copy-start(bf16[1,256,2048]{2,1,0:T(8,128)(2,1)} %param.16) | copy-start | bytes 3145732
  36.7 5.8 %copy-start.6 = (bf16[2048,128]{1,0:T(8,128)(2,1)S(1)}, bf16[2048,128]{1,0:T(8,128)(2,1)}, u32[]{:S(2)}) copy-start(bf16[2048,128]{1,0:T(8,128)(2,1)} %sg.1) | copy-start | bytes 1572868
  36.7 5.8 %copy-start.7 = (bf16[2048,128]{1,0:T(8,128)(2,1)S(1)}, bf16[2048,128]{1,0:T(8,128)(2,1)}, u32[]{:S(2)}) copy-start(bf16[2048,128]{1,0:T(8,128)(2,1)} %su.1) | copy-start | bytes 1572868
  36.7 5.8 %copy-start.8 = (bf16[128,2048]{1,0:T(8,128)(2,1)S(1)}, bf16[128,2048]{1,0:T(8,128)(2,1)}, u32[]{:S(2)}) copy-start(bf16[128,2048]{1,0:T(8,128)(2,1)} %sd.1) | copy-start | bytes 1572868
  36.7 11.3 %collective-permute-start.9 = (bf16[96,1024]{1,0:T(8,128)(2,1)S(1)}, bf16[96,1024]{1,0:T(8,128)(2,1)S(1)}, u32[]{:S(2)}, u32[]{:S(2)}) collective-permute-start(bf16[96,1024]{1,0:T(8,128)(2,1)S(1)} %get-tuple-element.45), channel_id=1, source_target_pairs={{0,2},{1,3},{2,0},{3,1},{4,6},{5,7},{6,4},{7,5},{8,10},{9,11},{10,... | collective-permute-start | bytes 589832 | tf_op jit(solution)/shard_map/ppermute | solution.py:71
  40.9 1.6 %copy-start.12 = (f32[256,2]{0,1:T(2,128)S(1)}, f32[256,2]{0,1:T(2,128)}, u32[]{:S(2)}) copy-start(f32[256,2]{0,1:T(2,128)} %param.13) | copy-start | bytes 6148
  40.9 1.6 %copy-start.10 = (s32[256,2]{0,1:T(2,128)S(1)}, s32[256,2]{0,1:T(2,128)}, u32[]{:S(2)}) copy-start(s32[256,2]{0,1:T(2,128)} %param.12) | copy-start | bytes 6148
  40.9 10.4 %collective-permute-start.5 = (bf16[96,1024]{1,0:T(8,128)(2,1)S(1)}, bf16[96,1024]{1,0:T(8,128)(2,1)S(1)}, u32[]{:S(2)}, u32[]{:S(2)}) collective-permute-start(bf16[96,1024]{1,0:T(8,128)(2,1)S(1)} %get-tuple-element.40), channel_id=1, source_target_pairs={{0,2},{1,3},{2,0},{3,1},{4,6},{5,7},{6,4},{7,5},{8,10},{9,11},{10,... | collective-permute-start | bytes 589832 | tf_op jit(solution)/shard_map/ppermute | solution.py:71
  45.0 6.4 %collective-permute-start.16 = (bf16[256,512]{1,0:T(8,128)(2,1)S(1)}, bf16[256,512]{1,0:T(8,128)(2,1)S(1)}, u32[]{:S(2)}, u32[]{:S(2)}) collective-permute-start(bf16[256,512]{1,0:T(8,128)(2,1)S(1)} %get-tuple-element.59), channel_id=1, source_target_pairs={{0,1},{1,0},{2,3},{3,2},{4,5},{5,4},{6,7},{7,6},{8,9},{9,8},{10,11... | collective-permute-start | bytes 786440 | tf_op jit(solution)/shard_map/ppermute | solution.py:71
  45.1 6.3 %collective-permute-start.17 = (bf16[256,512]{1,0:T(8,128)(2,1)S(1)}, bf16[256,512]{1,0:T(8,128)(2,1)S(1)}, u32[]{:S(2)}, u32[]{:S(2)}) collective-permute-start(bf16[256,512]{1,0:T(8,128)(2,1)S(1)} %get-tuple-element.60), channel_id=1, source_target_pairs={{0,1},{1,0},{2,3},{3,2},{4,5},{5,4},{6,7},{7,6},{8,9},{9,8},{10,11... | collective-permute-start | bytes 786440 | tf_op jit(solution)/shard_map/ppermute | solution.py:71
  45.6 8.6 %collective-permute-start.14 = (bf16[96,1024]{1,0:T(8,128)(2,1)S(1)}, bf16[96,1024]{1,0:T(8,128)(2,1)S(1)}, u32[]{:S(2)}, u32[]{:S(2)}) collective-permute-start(bf16[96,1024]{1,0:T(8,128)(2,1)S(1)} %shard_map.107), channel_id=1, source_target_pairs={{0,12},{4,0},{8,4},{12,8},{1,13},{5,1},{9,5},{13,9},{2,14},{6,2},{... | collective-permute-start | bytes 589832 | tf_op jit(solution)/shard_map/ppermute | solution.py:74
  48.1 16.1 %collective-permute-start.10 = (bf16[96,1024]{1,0:T(8,128)(2,1)S(1)}, bf16[96,1024]{1,0:T(8,128)(2,1)S(1)}, u32[]{:S(2)}, u32[]{:S(2)}) collective-permute-start(bf16[96,1024]{1,0:T(8,128)(2,1)S(1)} %shard_map.105), channel_id=1, source_target_pairs={{0,8},{4,12},{8,0},{12,4},{1,9},{5,13},{9,1},{13,5},{2,10},{6,14},... | collective-permute-start | bytes 589832 | tf_op jit(solution)/shard_map/ppermute | solution.py:74
  51.4 13.3 %collective-permute-start.6 = (bf16[96,1024]{1,0:T(8,128)(2,1)S(1)}, bf16[96,1024]{1,0:T(8,128)(2,1)S(1)}, u32[]{:S(2)}, u32[]{:S(2)}) collective-permute-start(bf16[96,1024]{1,0:T(8,128)(2,1)S(1)} %shard_map.103), channel_id=1, source_target_pairs={{0,4},{4,8},{8,12},{12,0},{1,5},{5,9},{9,13},{13,1},{2,6},{6,10},{... | collective-permute-start | bytes 589832 | tf_op jit(solution)/shard_map/ppermute | solution.py:74
  51.6 13.6 %collective-permute-start.18 = (bf16[256,512]{1,0:T(8,128)(2,1)S(1)}, bf16[256,512]{1,0:T(8,128)(2,1)S(1)}, u32[]{:S(2)}, u32[]{:S(2)}) collective-permute-start(bf16[256,512]{1,0:T(8,128)(2,1)S(1)} %get-tuple-element.62), channel_id=1, source_target_pairs={{0,2},{1,3},{2,0},{3,1},{4,6},{5,7},{6,4},{7,5},{8,10},{9,11},{10,... | collective-permute-start | bytes 786440 | tf_op jit(solution)/shard_map/ppermute | solution.py:71
  65.1 1.6 %collective-permute-start.15 = (bf16[256,512]{1,0:T(8,128)(2,1)S(1)}, bf16[256,512]{1,0:T(8,128)(2,1)S(1)}, u32[]{:S(2)}, u32[]{:S(2)}) collective-permute-start(bf16[256,512]{1,0:T(8,128)(2,1)S(1)} %get-tuple-element.56), channel_id=1, source_target_pairs={{0,1},{1,0},{2,3},{3,2},{4,5},{5,4},{6,7},{7,6},{8,9},{9,8},{10,11... | collective-permute-start | bytes 786440 | tf_op jit(solution)/shard_map/ppermute | solution.py:71

commit v2 on v1

--- a/solution.py
+++ b/solution.py
@@ -24,11 +24,12 @@
     return (gate / (1.0 + jnp.exp(-gate)) * up).astype(BF)
 
 
-def call(kernel, outs, args, mib=16, **more):
+def call(kernel, outs, args, loads=0, mib=16, **more):
     return pl.pallas_call(
         kernel,
         out_shape=outs,
-        in_specs=[pl.BlockSpec(memory_space=VM)] * len(args),
+        in_specs=[pl.BlockSpec(memory_space=VM)] * (len(args) - loads)
+        + [pl.BlockSpec(memory_space=pltpu.MemorySpace.HBM)] * loads,
         out_specs=jax.tree.map(lambda _: pl.BlockSpec(memory_space=VM), outs),
         compiler_params=pltpu.CompilerParams(vmem_limit_bytes=mib * 1024 * 1024),
         **more,
@@ -83,12 +84,26 @@
     near_gate, near_up = over_tp(w_gate, 1), over_tp(w_up, 1)
     near_down = over_tp(w_down, 1)
 
-    def dispatch(tokens_ref, gain_ref, routing_ref, normed_ref, *send_refs):
-        values = tokens_ref[...].astype(F32)
-        scale = lax.rsqrt(jnp.mean(values * values, axis=-1, keepdims=True) + 1e-06)
-        normed_ref[...] = (values * scale * gain_ref[...]).astype(BF)
+    blocks = 4
+    step = rows // blocks
+
+    def dispatch(tokens_hbm, gain_hbm, routing_hbm, normed_ref, *refs):
+        send_refs, (tokens_ref, gain_ref, routing_ref, sems) = refs[: len(order)], refs[len(order) :]
+        chunks = [pl.ds(i * step, step) for i in range(blocks)]
+        loads = [(routing_hbm, routing_ref), (gain_hbm, gain_ref)]
+        loads += [(tokens_hbm.at[c], tokens_ref.at[c]) for c in chunks]
+        copies = [pltpu.make_async_copy(src, dst, sems.at[i]) for i, (src, dst) in enumerate(loads)]
+        for copy in copies:
+            copy.start()
+        copies[0].wait()
         places = places_of(routing_ref[...], lax.axis_index("ep"), experts, capacity)
         places = [p.astype(jnp.int32) for p in places]
+        copies[1].wait()
+        for c, copy in zip(chunks, copies[2:]):
+            copy.wait()
+            values = tokens_ref[c, :].astype(F32)
+            scale = lax.rsqrt(jnp.mean(values * values, axis=-1, keepdims=True) + 1e-06)
+            normed_ref[c, :] = (values * scale * gain_ref[...]).astype(BF)
         mine = normed_ref[:, at_half(False)]
         base = (lax.axis_index("tp") % CORES) * part
         for send_ref, s in zip(send_refs, order):
@@ -103,18 +118,39 @@
         dispatch,
         [jax.ShapeDtypeStruct((rows, width), BF)] + [piece] * len(order),
         [tokens, norm_gain.reshape(1, width), routing],
+        loads=3,
+        scratch_shapes=[
+            pltpu.VMEM((rows, width), BF),
+            pltpu.VMEM((1, width), F32),
+            pltpu.VMEM((top, rows), jnp.int32),
+            pltpu.SemaphoreType.DMA((blocks + 2,)),
+        ],
     )
     arrived = [over_ep(x, s) for x, s in zip(sends, order)]
 
-    def local(normed_ref, routing_ref, gw_ref, wg, wu, wd, sg, su, sd, *refs):
-        out_refs, info_ref, pick_refs = refs[:tp_count], refs[tp_count], refs[tp_count + 1 :]
+    stored = [routing, gate_weights, w_gate, w_up, shared_gate, shared_up, w_down, shared_down]
+
+    def local(normed_ref, *refs):
+        sources, refs = refs[: len(stored)], refs[len(stored) :]
+        out_refs, info_ref, refs = refs[:tp_count], refs[tp_count], refs[tp_count + 1 :]
+        pick_refs, targets, sems = refs[: -len(stored) - 1], refs[-len(stored) - 1 : -1], refs[-1]
+        copies = [pltpu.make_async_copy(a, b, sems.at[i]) for i, (a, b) in enumerate(zip(sources, targets))]
+        for copy in copies:
+            copy.start()
+        routing_ref, gw_ref, wg, wu, sg, su, wd, sd = targets
+        copies[0].wait()
+        copies[1].wait()
         places = places_of(routing_ref[...], lax.axis_index("ep"), experts, capacity)
         index = lax.broadcasted_iota(jnp.int32, (capacity, rows), 0)
         own = (index == places[0].astype(jnp.int32)).astype(F32)
         for p in places[1:]:
             own = own + (index == p.astype(jnp.int32)).astype(F32)
         own_rows = dot(own.astype(BF), normed_ref[...]).astype(BF)
+        copies[2].wait()
+        copies[3].wait()
         hidden = swiglu(dot(own_rows, wg[...]), dot(own_rows, wu[...]))
+        copies[4].wait()
+        copies[5].wait()
         s_hidden = swiglu(dot(normed_ref[...], sg[...]), dot(normed_ref[...], su[...]))
         info = jnp.zeros((128, rows), F32)
         line = lax.broadcasted_iota(jnp.int32, (128, rows), 0)
@@ -132,6 +168,8 @@
             pick = pick + (columns[k] == lanes).astype(F32)
             weight = weight + jnp.where(columns[k] < capacity, weights[k], 0.0)
         pick = pick.astype(BF)
+        copies[6].wait()
+        copies[7].wait()
         for m in range(tp_count):
             term = dot(hidden, wd[:, at_quarter(m)]).astype(BF)
             shared = dot(s_hidden, sd[:, at_quarter(m)])
@@ -148,7 +186,9 @@
         [out_piece] * tp_count
         + [jax.ShapeDtypeStruct((rows, 128), F32)]
         + [jax.ShapeDtypeStruct((rows, part), BF)] * (top * len(order)),
-        [normed, routing, gate_weights, w_gate, w_up, w_down, shared_gate, shared_up, shared_down],
+        [normed, *stored],
+        loads=len(stored),
+        scratch_shapes=[pltpu.VMEM(x.shape, x.dtype) for x in stored] + [pltpu.SemaphoreType.DMA((len(stored),))],
     )
     info, picks = partials[tp_count], partials[tp_count + 1 :]
     partials = partials[:tp_count]

time: 67.8 us -> 69.2 us (1.021)
  Pallas kernels: 9.67 us -> 11.1 us
    pallas_call x13, Pallas kernels: 9.67 us -> 11.1 us  [call(): pl.pallas_call(kernel, out_shape=outs, in_specs=[pl.BlockSpec(memory_spac...]
    ppermute x13, waiting for transfers between devices: 6.53 us -> 5.45 us  [over_tp(): return lax.ppermute(x, 'tp', [(i, i ^ m) for i in range(tp_count)])]
    ppermute x6, waiting for transfers between devices: 26 us -> 27 us  [over_ep(): lax.ppermute(x, 'ep', [(i, (i + s) % ep_count) for i in range(ep_count)])]
  transfers between devices with their start and end apart: 19 -> 19, of which waited for: 9 -> 9; matrix products, arithmetic and copies ran while one was open for 0% -> 0% of each run, Pallas kernels for 13% -> 15%
where the time goes in v2:
time: 69.2 us; the launch traced here: 68.9 us
  waiting for transfers between devices  32.5 us (47%)
  starting transfers between devices  20 us (29%)
  Pallas kernels  11.1 us (16%)
  local copies, waits for them, and re-layouts  5.09 us (7%)
    ppermute x6, waiting for transfers between devices, over_ep(): lax.ppermute(x, 'ep', [(i, (i + s) % ep_count) for i in range(ep_count)])  27 us
    ppermute x13, starting transfers between devices, over_tp(): return lax.ppermute(x, 'tp', [(i, i ^ m) for i in range(tp_count)])  11.4 us
    pallas_call x13, Pallas kernels, call(): pl.pallas_call(kernel, out_shape=outs, in_specs=[pl.BlockSpec(memory_spac...  11.1 us
    ppermute x6, starting transfers between devices, over_ep(): lax.ppermute(x, 'ep', [(i, (i + s) % ep_count) for i in range(ep_count)])  8.59 us
    ppermute x13, waiting for transfers between devices, over_tp(): return lax.ppermute(x, 'tp', [(i, i ^ m) for i in range(tp_count)])  5.45 us
    unnamed x26, local copies, waits for them, and re-layouts  5.09 us
  transfers between devices with their start and end apart: 19, of which 9 were waited for; matrix products, arithmetic and copies ran while one was open for 0% of the time, Pallas kernels for 15%

profile of v2, /device:TPU:0, one launch (start us, length us, event | category | flops | bytes accessed | tf_op | source)
XLA Modules:
  0.0 68.9 jit_solution(2343567651126983825)
XLA Ops:
  0.0 0.5 collective-permute-start.2
  0.5 0.1 collective-permute-start.3
  0.6 0.4 collective-permute-start.4
  1.0 1.2 %copy-done.5 = bf16[256,2048]{1,0:T(8,128)(2,1)S(1)} copy-done((bf16[256,2048]{1,0:T(8,128)(2,1)S(1)}, bf16[256,2048]{1,0:T(8,128)(2,1)}, u32[]{:S(2)}) %copy-start.5) | copy-done | bytes 1048600
  2.2 0.7 copy-done.9
  2.9 0.7 %copy-done.11 = f32[2048]{0:T(1024)S(1)} copy-done((f32[2048]{0:T(1024)S(1)}, f32[2048]{0:T(1024)}, u32[]{:S(2)}) %copy-start.11) | copy-done | bytes 8216
  3.6 1.4 %shard_map.100 = (bf16[256,2048]{1,0:T(8,128)(2,1)S(1)}, bf16[96,1024]{1,0:T(8,128)(2,1)S(1)}, bf16[96,1024]{1,0:T(8,128)(2,1)S(1)}, bf16[96,1024]{1,0:T(8,128)(2,1)S(1)}) custom-call(bf16[256,2048]{1,0:T(8,128)(2,1)S(1)} %copy-done.5, f32[1,2048]{1,0:T(1,128)S(1)} %bitcast.23, s32[2,256]{1,0:T(2,128)S(1)} %bitcast.21), custom_call_target="tpu_custom_call" | custom-call | tf_op jit(solution)/shard_map/pallas_call | solution.py:28
  5.0 4.7 %collective-permute-start = (bf16[96,1024]{1,0:T(8,128)(2,1)S(1)}, bf16[96,1024]{1,0:T(8,128)(2,1)S(1)}, u32[]{:S(2)}, u32[]{:S(2)}) collective-permute-start(bf16[96,1024]{1,0:T(8,128)(2,1)S(1)} %get-tuple-element.38), channel_id=1, source_target_pairs={{0,12},{4,0},{8,4},{12,8},{1,13},{5,1},{9,5},{13,9},{2,14},{6,2},{... | collective-permute-start | bytes 589832 | tf_op jit(solution)/shard_map/ppermute | solution.py:75
  9.7 5.3 %collective-permute-done.refs_0_ = bf16[96,1024]{1,0:T(8,128)(2,1)S(1)} collective-permute-done((bf16[96,1024]{1,0:T(8,128)(2,1)S(1)}, bf16[96,1024]{1,0:T(8,128)(2,1)S(1)}, u32[]{:S(2)}, u32[]{:S(2)}) %collective-permute-start) | collective-permute-done | bytes 196640 | tf_op jit(solution)/shard_map/ppermute | solution.py:75
  15.0 1.4 %collective-permute-start.7 = (bf16[96,1024]{1,0:T(8,128)(2,1)S(1)}, bf16[96,1024]{1,0:T(8,128)(2,1)S(1)}, u32[]{:S(2)}, u32[]{:S(2)}) collective-permute-start(bf16[96,1024]{1,0:T(8,128)(2,1)S(1)} %get-tuple-element.43), channel_id=1, source_target_pairs={{0,8},{4,12},{8,0},{12,4},{1,9},{5,13},{9,1},{13,5},{2,10},{6,14},... | collective-permute-start | bytes 589832 | tf_op jit(solution)/shard_map/ppermute | solution.py:75
  16.4 3.6 %collective-permute-done.11.refs_0_ = bf16[96,1024]{1,0:T(8,128)(2,1)S(1)} collective-permute-done((bf16[96,1024]{1,0:T(8,128)(2,1)S(1)}, bf16[96,1024]{1,0:T(8,128)(2,1)S(1)}, u32[]{:S(2)}, u32[]{:S(2)}) %collective-permute-start.11) | collective-permute-done | bytes 196640 | tf_op jit(solution)/shard_map/ppermute | solution.py:75
  20.0 1.5 %collective-permute-start.12 = (bf16[96,1024]{1,0:T(8,128)(2,1)S(1)}, bf16[96,1024]{1,0:T(8,128)(2,1)S(1)}, u32[]{:S(2)}, u32[]{:S(2)}) collective-permute-start(bf16[96,1024]{1,0:T(8,128)(2,1)S(1)} %collective-permute-done.11.refs_0_), channel_id=1, source_target_pairs={{0,2},{1,3},{2,0},{3,1},{4,6},{5,7},{6,4},{7,5},{8,10},{9,11},{10,... | collective-permute-start | bytes 589832 | tf_op jit(solution)/shard_map/ppermute | solution.py:72
  21.5 6.5 %collective-permute-done.7.refs_0_ = bf16[96,1024]{1,0:T(8,128)(2,1)S(1)} collective-permute-done((bf16[96,1024]{1,0:T(8,128)(2,1)S(1)}, bf16[96,1024]{1,0:T(8,128)(2,1)S(1)}, u32[]{:S(2)}, u32[]{:S(2)}) %collective-permute-start.7) | collective-permute-done | bytes 196640 | tf_op jit(solution)/shard_map/ppermute | solution.py:75
  28.0 1.5 %collective-permute-start.8 = (bf16[96,1024]{1,0:T(8,128)(2,1)S(1)}, bf16[96,1024]{1,0:T(8,128)(2,1)S(1)}, u32[]{:S(2)}, u32[]{:S(2)}) collective-permute-start(bf16[96,1024]{1,0:T(8,128)(2,1)S(1)} %collective-permute-done.7.refs_0_), channel_id=1, source_target_pairs={{0,2},{1,3},{2,0},{3,1},{4,6},{5,7},{6,4},{7,5},{8,10},{9,11},{10,... | collective-permute-start | bytes 589832 | tf_op jit(solution)/shard_map/ppermute | solution.py:72
  29.5 0.5 collective-permute-start.1
  30.0 0.0 copy-start.1
  30.1 1.2 %copy-done.1 = bf16[1,2048,256]{2,1,0:T(8,128)(2,1)S(1)} copy-done((bf16[1,2048,256]{2,1,0:T(8,128)(2,1)S(1)}, bf16[1,2048,256]{2,1,0:T(8,128)(2,1)}, u32[]{:S(2)}) %copy-start.1) | copy-done | bytes 1048600
  31.3 1.2 %copy-done.3 = bf16[1,256,2048]{2,1,0:T(8,128)(2,1)S(1)} copy-done((bf16[1,256,2048]{2,1,0:T(8,128)(2,1)S(1)}, bf16[1,256,2048]{2,1,0:T(8,128)(2,1)}, u32[]{:S(2)}) %copy-start.3) | copy-done | bytes 1048600
  32.5 1.2 %shard_map.106 = (bf16[96,1024]{1,0:T(8,128)(2,1)S(1)}, bf16[96,1024]{1,0:T(8,128)(2,1)S(1)}) custom-call(bf16[96,1024]{1,0:T(8,128)(2,1)S(1)} %collective-permute-done.11.refs_0_, bf16[96,1024]{1,0:T(8,128)(2,1)S(1)} %collective-permute-done.12.refs_1_, bf16[2048,256]{1,0:T(8,128)(2,1)S(1)} %bitcast.7, bf16[2048,256]{1,0:T(8,128)(2,1)S(1)} %bitcast.12, ...), custom_call_target="tpu_custom_call" | custom-call | tf_op jit(solution)/shard_map/pallas_call | solution.py:28
  33.7 1.6 %collective-permute-start.13 = (bf16[96,1024]{1,0:T(8,128)(2,1)S(1)}, bf16[96,1024]{1,0:T(8,128)(2,1)S(1)}, u32[]{:S(2)}, u32[]{:S(2)}) collective-permute-start(bf16[96,1024]{1,0:T(8,128)(2,1)S(1)} %get-tuple-element.50), channel_id=1, source_target_pairs={{0,2},{1,3},{2,0},{3,1},{4,6},{5,7},{6,4},{7,5},{8,10},{9,11},{10,... | collective-permute-start | bytes 589832 | tf_op jit(solution)/shard_map/ppermute | solution.py:72
  35.3 0.5 collective-permute-done.8.refs_1_
  35.8 1.2 %shard_map.104 = (bf16[96,1024]{1,0:T(8,128)(2,1)S(1)}, bf16[96,1024]{1,0:T(8,128)(2,1)S(1)}) custom-call(bf16[96,1024]{1,0:T(8,128)(2,1)S(1)} %collective-permute-done.7.refs_0_, bf16[96,1024]{1,0:T(8,128)(2,1)S(1)} %collective-permute-done.8.refs_1_, bf16[2048,256]{1,0:T(8,128)(2,1)S(1)} %bitcast.8, bf16[2048,256]{1,0:T(8,128)(2,1)S(1)} %bitcast.13, ...), custom_call_target="tpu_custom_call" | custom-call | tf_op jit(solution)/shard_map/pallas_call | solution.py:28
  37.0 0.0 copy-start.2
  37.0 0.0 copy-start.4
  37.0 0.0 copy-start.7
  37.1 0.0 copy-start.8
  37.1 1.6 %collective-permute-start.9 = (bf16[96,1024]{1,0:T(8,128)(2,1)S(1)}, bf16[96,1024]{1,0:T(8,128)(2,1)S(1)}, u32[]{:S(2)}, u32[]{:S(2)}) collective-permute-start(bf16[96,1024]{1,0:T(8,128)(2,1)S(1)} %get-tuple-element.45), channel_id=1, source_target_pairs={{0,2},{1,3},{2,0},{3,1},{4,6},{5,7},{6,4},{7,5},{8,10},{9,11},{10,... | collective-permute-start | bytes 589832 | tf_op jit(solution)/shard_map/ppermute | solution.py:72
  38.6 1.3 %collective-permute-done.1.refs_1_ = bf16[96,1024]{1,0:T(8,128)(2,1)S(1)} collective-permute-done((bf16[96,1024]{1,0:T(8,128)(2,1)S(1)}, bf16[96,1024]{1,0:T(8,128)(2,1)S(1)}, u32[]{:S(2)}, u32[]{:S(2)}) %collective-permute-start.1) | collective-permute-done | bytes 196640 | tf_op jit(solution)/shard_map/ppermute | solution.py:72
  40.0 1.3 %shard_map.102 = (bf16[96,1024]{1,0:T(8,128)(2,1)S(1)}, bf16[96,1024]{1,0:T(8,128)(2,1)S(1)}) custom-call(bf16[96,1024]{1,0:T(8,128)(2,1)S(1)} %collective-permute-done.refs_0_, bf16[96,1024]{1,0:T(8,128)(2,1)S(1)} %collective-permute-done.1.refs_1_, bf16[2048,256]{1,0:T(8,128)(2,1)S(1)} %bitcast.9, bf16[2048,256]{1,0:T(8,128)(2,1)S(1)} %bitcast.14, ...), custom_call_target="tpu_custom_call" | custom-call | tf_op jit(solution)/shard_map/pallas_call | solution.py:28
  41.2 0.0 copy-start.10
  41.3 1.6 %collective-permute-start.5 = (bf16[96,1024]{1,0:T(8,128)(2,1)S(1)}, bf16[96,1024]{1,0:T(8,128)(2,1)S(1)}, u32[]{:S(2)}, u32[]{:S(2)}) collective-permute-start(bf16[96,1024]{1,0:T(8,128)(2,1)S(1)} %get-tuple-element.40), channel_id=1, source_target_pairs={{0,2},{1,3},{2,0},{3,1},{4,6},{5,7},{6,4},{7,5},{8,10},{9,11},{10,... | collective-permute-start | bytes 589832 | tf_op jit(solution)/shard_map/ppermute | solution.py:72
  42.9 3.6 %shard_map.101 = (bf16[256,512]{1,0:T(8,128)(2,1)S(1)}, bf16[256,512]{1,0:T(8,128)(2,1)S(1)}, bf16[256,512]{1,0:T(8,128)(2,1)S(1)}, bf16[256,512]{1,0:T(8,128)(2...) custom-call(bf16[256,2048]{1,0:T(8,128)(2,1)S(1)} %get-tuple-element, ...), custom_call_target="tpu_custom_call" | custom-call | tf_op jit(solution)/shard_map/pallas_call | solution.py:28
  46.4 0.1 collective-permute-start.16
  46.5 0.5 collective-permute-start.17
  47.1 2.3 %collective-permute-start.14 = (bf16[96,1024]{1,0:T(8,128)(2,1)S(1)}, bf16[96,1024]{1,0:T(8,128)(2,1)S(1)}, u32[]{:S(2)}, u32[]{:S(2)}) collective-permute-start(bf16[96,1024]{1,0:T(8,128)(2,1)S(1)} %shard_map.107), channel_id=1, source_target_pairs={{0,12},{4,0},{8,4},{12,8},{1,13},{5,1},{9,5},{13,9},{2,14},{6,2},{... | collective-permute-start | bytes 589832 | tf_op jit(solution)/shard_map/ppermute | solution.py:75
  49.5 0.1 collective-permute-start.10
  49.5 2.1 %collective-permute-done.5.refs_1_ = bf16[96,1024]{1,0:T(8,128)(2,1)S(1)} collective-permute-done((bf16[96,1024]{1,0:T(8,128)(2,1)S(1)}, bf16[96,1024]{1,0:T(8,128)(2,1)S(1)}, u32[]{:S(2)}, u32[]{:S(2)}) %collective-permute-start.5) | collective-permute-done | bytes 196640 | tf_op jit(solution)/shard_map/ppermute | solution.py:72
  51.7 0.1 collective-permute-start.6
  51.8 0.1 shard_map.111
  51.9 1.6 %collective-permute-start.18 = (bf16[256,512]{1,0:T(8,128)(2,1)S(1)}, bf16[256,512]{1,0:T(8,128)(2,1)S(1)}, u32[]{:S(2)}, u32[]{:S(2)}) collective-permute-start(bf16[256,512]{1,0:T(8,128)(2,1)S(1)} %get-tuple-element.62), channel_id=1, source_target_pairs={{0,2},{1,3},{2,0},{3,1},{4,6},{5,7},{6,4},{7,5},{8,10},{9,11},{10,... | collective-permute-start | bytes 786440 | tf_op jit(solution)/shard_map/ppermute | solution.py:72
  53.5 2.2 %collective-permute-done.14.refs_2_ = bf16[96,1024]{1,0:T(8,128)(2,1)S(1)} collective-permute-done((bf16[96,1024]{1,0:T(8,128)(2,1)S(1)}, bf16[96,1024]{1,0:T(8,128)(2,1)S(1)}, u32[]{:S(2)}, u32[]{:S(2)}) %collective-permute-start.14) | collective-permute-done | bytes 196640 | tf_op jit(solution)/shard_map/ppermute | solution.py:75
  55.7 0.4 shard_map.108
  56.2 9.4 %collective-permute-done.10.refs_2_ = bf16[96,1024]{1,0:T(8,128)(2,1)S(1)} collective-permute-done((bf16[96,1024]{1,0:T(8,128)(2,1)S(1)}, bf16[96,1024]{1,0:T(8,128)(2,1)S(1)}, u32[]{:S(2)}, u32[]{:S(2)}) %collective-permute-start.10) | collective-permute-done | bytes 196640 | tf_op jit(solution)/shard_map/ppermute | solution.py:75
  65.6 0.5 shard_map.109
  66.0 0.5 shard_map.110
  66.5 0.1 collective-permute-start.15
  66.6 1.5 %collective-permute-done.15.more_ref = bf16[256,512]{1,0:T(8,128)(2,1)S(1)} collective-permute-done((bf16[256,512]{1,0:T(8,128)(2,1)S(1)}, bf16[256,512]{1,0:T(8,128)(2,1)S(1)}, u32[]{:S(2)}, u32[]{:S(2)}) %collective-permute-start.15) | collective-permute-done | bytes 262176 | tf_op jit(solution)/shard_map/ppermute | solution.py:72
  68.1 0.8 %shard_map.112 = bf16[256,512]{1,0:T(8,128)(2,1)} custom-call(f32[256,512]{1,0:T(8,128)S(1)} %get-tuple-element.55.mine_ref, bf16[256,512]{1,0:T(8,128)(2,1)S(1)} %collective-permute-done.15.more_ref, bf16[256,512]{1,0:T(8,128)(2,1)S(1)} %get-tuple-element.61.near_ref, bf16[256,512]{1,0:T(8,128)(2,1)S(1)} %collective-permute-done.18.far_ref), custom_call_target="tpu_custom_call" | custom-call | tf_op jit(solution)/shard_map/pallas_call | solution.py:28
  (29 shorter events, 0.2 us)
Async XLA Ops:
  0.0 30.0 %copy-start = (bf16[1,2048,256]{2,1,0:T(8,128)(2,1)S(1)}, bf16[1,2048,256]{2,1,0:T(8,128)(2,1)}, u32[]{:S(2)}) copy-start(bf16[1,2048,256]{2,1,0:T(8,128)(2,1)} %param.14) | copy-start | bytes 3145732
  0.0 30.0 %collective-permute-start.2 = (bf16[2048,256]{1,0:T(8,128)(2,1)}, bf16[2048,256]{1,0:T(8,128)(2,1)S(1)}, u32[]{:S(2)}, u32[]{:S(2)}) collective-permute-start(bf16[2048,256]{1,0:T(8,128)(2,1)} %bitcast.6), channel_id=1, source_target_pairs={{0,1},{1,0},{2,3},{3,2},{4,5},{5,4},{6,7},{7,6},{8,9},{9,8},{10,11... | collective-permute-start | bytes 3145736 | tf_op jit(solution)/shard_map/ppermute | solution.py:72
  0.5 29.5 %collective-permute-start.3 = (bf16[2048,256]{1,0:T(8,128)(2,1)}, bf16[2048,256]{1,0:T(8,128)(2,1)S(1)}, u32[]{:S(2)}, u32[]{:S(2)}) collective-permute-start(bf16[2048,256]{1,0:T(8,128)(2,1)} %bitcast.11), channel_id=1, source_target_pairs={{0,1},{1,0},{2,3},{3,2},{4,5},{5,4},{6,7},{7,6},{8,9},{9,8},{10,11... | collective-permute-start | bytes 3145736 | tf_op jit(solution)/shard_map/ppermute | solution.py:72
  0.6 29.5 %collective-permute-start.4 = (bf16[256,2048]{1,0:T(8,128)(2,1)}, bf16[256,2048]{1,0:T(8,128)(2,1)S(1)}, u32[]{:S(2)}, u32[]{:S(2)}) collective-permute-start(bf16[256,2048]{1,0:T(8,128)(2,1)} %bitcast.16), channel_id=1, source_target_pairs={{0,1},{1,0},{2,3},{3,2},{4,5},{5,4},{6,7},{7,6},{8,9},{9,8},{10,11... | collective-permute-start | bytes 3145736 | tf_op jit(solution)/shard_map/ppermute | solution.py:72
  1.0 1.2 %copy-start.5 = (bf16[256,2048]{1,0:T(8,128)(2,1)S(1)}, bf16[256,2048]{1,0:T(8,128)(2,1)}, u32[]{:S(2)}) copy-start(bf16[256,2048]{1,0:T(8,128)(2,1)} %tokens_hbm.1) | copy-start | bytes 3145732
  2.2 0.7 copy-start.9
  2.9 0.7 %copy-start.11 = (f32[2048]{0:T(1024)S(1)}, f32[2048]{0:T(1024)}, u32[]{:S(2)}) copy-start(f32[2048]{0:T(1024)} %param.11) | copy-start | bytes 24580
  5.0 10.0 %collective-permute-start = (bf16[96,1024]{1,0:T(8,128)(2,1)S(1)}, bf16[96,1024]{1,0:T(8,128)(2,1)S(1)}, u32[]{:S(2)}, u32[]{:S(2)}) collective-permute-start(bf16[96,1024]{1,0:T(8,128)(2,1)S(1)} %get-tuple-element.38), channel_id=1, source_target_pairs={{0,12},{4,0},{8,4},{12,8},{1,13},{5,1},{9,5},{13,9},{2,14},{6,2},{... | collective-permute-start | bytes 589832 | tf_op jit(solution)/shard_map/ppermute | solution.py:75
  9.7 10.4 %collective-permute-start.11 = (bf16[96,1024]{1,0:T(8,128)(2,1)S(1)}, bf16[96,1024]{1,0:T(8,128)(2,1)S(1)}, u32[]{:S(2)}, u32[]{:S(2)}) collective-permute-start(bf16[96,1024]{1,0:T(8,128)(2,1)S(1)} %get-tuple-element.48), channel_id=1, source_target_pairs={{0,4},{4,8},{8,12},{12,0},{1,5},{5,9},{9,13},{13,1},{2,6},{6,10},{... | collective-permute-start | bytes 589832 | tf_op jit(solution)/shard_map/ppermute | solution.py:75
  15.0 13.0 %collective-permute-start.7 = (bf16[96,1024]{1,0:T(8,128)(2,1)S(1)}, bf16[96,1024]{1,0:T(8,128)(2,1)S(1)}, u32[]{:S(2)}, u32[]{:S(2)}) collective-permute-start(bf16[96,1024]{1,0:T(8,128)(2,1)S(1)} %get-tuple-element.43), channel_id=1, source_target_pairs={{0,8},{4,12},{8,0},{12,4},{1,9},{5,13},{9,1},{13,5},{2,10},{6,14},... | collective-permute-start | bytes 589832 | tf_op jit(solution)/shard_map/ppermute | solution.py:75
  20.0 9.5 %collective-permute-start.12 = (bf16[96,1024]{1,0:T(8,128)(2,1)S(1)}, bf16[96,1024]{1,0:T(8,128)(2,1)S(1)}, u32[]{:S(2)}, u32[]{:S(2)}) collective-permute-start(bf16[96,1024]{1,0:T(8,128)(2,1)S(1)} %collective-permute-done.11.refs_0_), channel_id=1, source_target_pairs={{0,2},{1,3},{2,0},{3,1},{4,6},{5,7},{6,4},{7,5},{8,10},{9,11},{10,... | collective-permute-start | bytes 589832 | tf_op jit(solution)/shard_map/ppermute | solution.py:72
  28.0 7.8 %collective-permute-start.8 = (bf16[96,1024]{1,0:T(8,128)(2,1)S(1)}, bf16[96,1024]{1,0:T(8,128)(2,1)S(1)}, u32[]{:S(2)}, u32[]{:S(2)}) collective-permute-start(bf16[96,1024]{1,0:T(8,128)(2,1)S(1)} %collective-permute-done.7.refs_0_), channel_id=1, source_target_pairs={{0,2},{1,3},{2,0},{3,1},{4,6},{5,7},{6,4},{7,5},{8,10},{9,11},{10,... | collective-permute-start | bytes 589832 | tf_op jit(solution)/shard_map/ppermute | solution.py:72
  29.5 10.5 %collective-permute-start.1 = (bf16[96,1024]{1,0:T(8,128)(2,1)S(1)}, bf16[96,1024]{1,0:T(8,128)(2,1)S(1)}, u32[]{:S(2)}, u32[]{:S(2)}) collective-permute-start(bf16[96,1024]{1,0:T(8,128)(2,1)S(1)} %collective-permute-done.refs_0_), channel_id=1, source_target_pairs={{0,2},{1,3},{2,0},{3,1},{4,6},{5,7},{6,4},{7,5},{8,10},{9,11},{10,... | collective-permute-start | bytes 589832 | tf_op jit(solution)/shard_map/ppermute | solution.py:72
  30.0 1.2 %copy-start.1 = (bf16[1,2048,256]{2,1,0:T(8,128)(2,1)S(1)}, bf16[1,2048,256]{2,1,0:T(8,128)(2,1)}, u32[]{:S(2)}) copy-start(bf16[1,2048,256]{2,1,0:T(8,128)(2,1)} %param.15) | copy-start | bytes 3145732
  31.3 1.2 %copy-start.3 = (bf16[1,256,2048]{2,1,0:T(8,128)(2,1)S(1)}, bf16[1,256,2048]{2,1,0:T(8,128)(2,1)}, u32[]{:S(2)}) copy-start(bf16[1,256,2048]{2,1,0:T(8,128)(2,1)} %param.16) | copy-start | bytes 3145732
  33.7 13.3 %collective-permute-start.13 = (bf16[96,1024]{1,0:T(8,128)(2,1)S(1)}, bf16[96,1024]{1,0:T(8,128)(2,1)S(1)}, u32[]{:S(2)}, u32[]{:S(2)}) collective-permute-start(bf16[96,1024]{1,0:T(8,128)(2,1)S(1)} %get-tuple-element.50), channel_id=1, source_target_pairs={{0,2},{1,3},{2,0},{3,1},{4,6},{5,7},{6,4},{7,5},{8,10},{9,11},{10,... | collective-permute-start | bytes 589832 | tf_op jit(solution)/shard_map/ppermute | solution.py:72
  37.0 5.8 %copy-start.2 = (bf16[1,2048,256]{2,1,0:T(8,128)(2,1)S(1)}, bf16[1,2048,256]{2,1,0:T(8,128)(2,1)}, u32[]{:S(2)}) copy-start(bf16[1,2048,256]{2,1,0:T(8,128)(2,1)} %param.15) | copy-start | bytes 3145732
  37.0 5.8 %copy-start.4 = (bf16[1,256,2048]{2,1,0:T(8,128)(2,1)S(1)}, bf16[1,256,2048]{2,1,0:T(8,128)(2,1)}, u32[]{:S(2)}) copy-start(bf16[1,256,2048]{2,1,0:T(8,128)(2,1)} %param.16) | copy-start | bytes 3145732
  37.0 5.8 %copy-start.6 = (bf16[2048,128]{1,0:T(8,128)(2,1)S(1)}, bf16[2048,128]{1,0:T(8,128)(2,1)}, u32[]{:S(2)}) copy-start(bf16[2048,128]{1,0:T(8,128)(2,1)} %refs_4_.1) | copy-start | bytes 1572868
  37.0 5.8 %copy-start.7 = (bf16[2048,128]{1,0:T(8,128)(2,1)S(1)}, bf16[2048,128]{1,0:T(8,128)(2,1)}, u32[]{:S(2)}) copy-start(bf16[2048,128]{1,0:T(8,128)(2,1)} %refs_5_.1) | copy-start | bytes 1572868
  37.1 5.8 %copy-start.8 = (bf16[128,2048]{1,0:T(8,128)(2,1)S(1)}, bf16[128,2048]{1,0:T(8,128)(2,1)}, u32[]{:S(2)}) copy-start(bf16[128,2048]{1,0:T(8,128)(2,1)} %refs_7_.1) | copy-start | bytes 1572868
  37.1 12.3 %collective-permute-start.9 = (bf16[96,1024]{1,0:T(8,128)(2,1)S(1)}, bf16[96,1024]{1,0:T(8,128)(2,1)S(1)}, u32[]{:S(2)}, u32[]{:S(2)}) collective-permute-start(bf16[96,1024]{1,0:T(8,128)(2,1)S(1)} %get-tuple-element.45), channel_id=1, source_target_pairs={{0,2},{1,3},{2,0},{3,1},{4,6},{5,7},{6,4},{7,5},{8,10},{9,11},{10,... | collective-permute-start | bytes 589832 | tf_op jit(solution)/shard_map/ppermute | solution.py:72
  41.2 1.6 %copy-start.12 = (f32[256,2]{0,1:T(2,128)S(1)}, f32[256,2]{0,1:T(2,128)}, u32[]{:S(2)}) copy-start(f32[256,2]{0,1:T(2,128)} %param.13) | copy-start | bytes 6148
  41.2 1.6 %copy-start.10 = (s32[256,2]{0,1:T(2,128)S(1)}, s32[256,2]{0,1:T(2,128)}, u32[]{:S(2)}) copy-start(s32[256,2]{0,1:T(2,128)} %param.12) | copy-start | bytes 6148
  41.3 10.4 %collective-permute-start.5 = (bf16[96,1024]{1,0:T(8,128)(2,1)S(1)}, bf16[96,1024]{1,0:T(8,128)(2,1)S(1)}, u32[]{:S(2)}, u32[]{:S(2)}) collective-permute-start(bf16[96,1024]{1,0:T(8,128)(2,1)S(1)} %get-tuple-element.40), channel_id=1, source_target_pairs={{0,2},{1,3},{2,0},{3,1},{4,6},{5,7},{6,4},{7,5},{8,10},{9,11},{10,... | collective-permute-start | bytes 589832 | tf_op jit(solution)/shard_map/ppermute | solution.py:72
  46.4 5.3 %collective-permute-start.16 = (bf16[256,512]{1,0:T(8,128)(2,1)S(1)}, bf16[256,512]{1,0:T(8,128)(2,1)S(1)}, u32[]{:S(2)}, u32[]{:S(2)}) collective-permute-start(bf16[256,512]{1,0:T(8,128)(2,1)S(1)} %get-tuple-element.59), channel_id=1, source_target_pairs={{0,1},{1,0},{2,3},{3,2},{4,5},{5,4},{6,7},{7,6},{8,9},{9,8},{10,11... | collective-permute-start | bytes 786440 | tf_op jit(solution)/shard_map/ppermute | solution.py:72
  46.5 5.3 %collective-permute-start.17 = (bf16[256,512]{1,0:T(8,128)(2,1)S(1)}, bf16[256,512]{1,0:T(8,128)(2,1)S(1)}, u32[]{:S(2)}, u32[]{:S(2)}) collective-permute-start(bf16[256,512]{1,0:T(8,128)(2,1)S(1)} %get-tuple-element.60), channel_id=1, source_target_pairs={{0,1},{1,0},{2,3},{3,2},{4,5},{5,4},{6,7},{7,6},{8,9},{9,8},{10,11... | collective-permute-start | bytes 786440 | tf_op jit(solution)/shard_map/ppermute | solution.py:72
  47.1 8.7 %collective-permute-start.14 = (bf16[96,1024]{1,0:T(8,128)(2,1)S(1)}, bf16[96,1024]{1,0:T(8,128)(2,1)S(1)}, u32[]{:S(2)}, u32[]{:S(2)}) collective-permute-start(bf16[96,1024]{1,0:T(8,128)(2,1)S(1)} %shard_map.107), channel_id=1, source_target_pairs={{0,12},{4,0},{8,4},{12,8},{1,13},{5,1},{9,5},{13,9},{2,14},{6,2},{... | collective-permute-start | bytes 589832 | tf_op jit(solution)/shard_map/ppermute | solution.py:75
  49.5 16.1 %collective-permute-start.10 = (bf16[96,1024]{1,0:T(8,128)(2,1)S(1)}, bf16[96,1024]{1,0:T(8,128)(2,1)S(1)}, u32[]{:S(2)}, u32[]{:S(2)}) collective-permute-start(bf16[96,1024]{1,0:T(8,128)(2,1)S(1)} %shard_map.105), channel_id=1, source_target_pairs={{0,8},{4,12},{8,0},{12,4},{1,9},{5,13},{9,1},{13,5},{2,10},{6,14},... | collective-permute-start | bytes 589832 | tf_op jit(solution)/shard_map/ppermute | solution.py:75
  51.7 14.3 %collective-permute-start.6 = (bf16[96,1024]{1,0:T(8,128)(2,1)S(1)}, bf16[96,1024]{1,0:T(8,128)(2,1)S(1)}, u32[]{:S(2)}, u32[]{:S(2)}) collective-permute-start(bf16[96,1024]{1,0:T(8,128)(2,1)S(1)} %shard_map.103), channel_id=1, source_target_pairs={{0,4},{4,8},{8,12},{12,0},{1,5},{5,9},{9,13},{13,1},{2,6},{6,10},{... | collective-permute-start | bytes 589832 | tf_op jit(solution)/shard_map/ppermute | solution.py:75
  51.9 14.6 %collective-permute-start.18 = (bf16[256,512]{1,0:T(8,128)(2,1)S(1)}, bf16[256,512]{1,0:T(8,128)(2,1)S(1)}, u32[]{:S(2)}, u32[]{:S(2)}) collective-permute-start(bf16[256,512]{1,0:T(8,128)(2,1)S(1)} %get-tuple-element.62), channel_id=1, source_target_pairs={{0,2},{1,3},{2,0},{3,1},{4,6},{5,7},{6,4},{7,5},{8,10},{9,11},{10,... | collective-permute-start | bytes 786440 | tf_op jit(solution)/shard_map/ppermute | solution.py:72
  66.5 1.6 %collective-permute-start.15 = (bf16[256,512]{1,0:T(8,128)(2,1)S(1)}, bf16[256,512]{1,0:T(8,128)(2,1)S(1)}, u32[]{:S(2)}, u32[]{:S(2)}) collective-permute-start(bf16[256,512]{1,0:T(8,128)(2,1)S(1)} %get-tuple-element.56), channel_id=1, source_target_pairs={{0,1},{1,0},{2,3},{3,2},{4,5},{5,4},{6,7},{7,6},{8,9},{9,8},{10,11... | collective-permute-start | bytes 786440 | tf_op jit(solution)/shard_map/ppermute | solution.py:72

commit v3 on v2

--- a/solution.py
+++ b/solution.py
@@ -25,6 +25,8 @@
 
 
 def call(kernel, outs, args, loads=0, mib=16, **more):
+    first = len(args) - loads
+    args = [pltpu.with_memory_space_constraint(x, pltpu.HBM) if i >= first else x for i, x in enumerate(args)]
     return pl.pallas_call(
         kernel,
         out_shape=outs,
@@ -64,6 +66,7 @@
     quarter = width // tp_count
     half = width // 2
     part = capacity // CORES
+    hid = expert_gate.shape[2]
     w_gate, w_up, w_down = expert_gate[0], expert_up[0], expert_down[0]
     order = shift_order(ep_count)
     routing, gate_weights = routing.T, gate_weights.T
@@ -87,11 +90,12 @@
     blocks = 4
     step = rows // blocks
 
-    def dispatch(tokens_hbm, gain_hbm, routing_hbm, normed_ref, *refs):
+    def dispatch(tokens_hbm, gain_hbm, routing_hbm, down_hbm, normed_ref, far_ref, *refs):
         send_refs, (tokens_ref, gain_ref, routing_ref, sems) = refs[: len(order)], refs[len(order) :]
         chunks = [pl.ds(i * step, step) for i in range(blocks)]
         loads = [(routing_hbm, routing_ref), (gain_hbm, gain_ref)]
         loads += [(tokens_hbm.at[c], tokens_ref.at[c]) for c in chunks]
+        loads += [(down_hbm.at[:, at_half(True)], far_ref)]
         copies = [pltpu.make_async_copy(src, dst, sems.at[i]) for i, (src, dst) in enumerate(loads)]
         for copy in copies:
             copy.start()
@@ -99,7 +103,7 @@
         places = places_of(routing_ref[...], lax.axis_index("ep"), experts, capacity)
         places = [p.astype(jnp.int32) for p in places]
         copies[1].wait()
-        for c, copy in zip(chunks, copies[2:]):
+        for c, copy in zip(chunks, copies[2:-1]):
             copy.wait()
             values = tokens_ref[c, :].astype(F32)
             scale = lax.rsqrt(jnp.mean(values * values, axis=-1, keepdims=True) + 1e-06)
@@ -112,20 +116,23 @@
             for p in places[1:]:
                 pick = pick + (index == p).astype(F32)
             send_ref[...] = dot(pick.astype(BF), mine).astype(BF)
+        copies[-1].wait()
 
     piece = jax.ShapeDtypeStruct((part, half), BF)
-    normed, *sends = call(
+    normed, far_half, *sends = call(
         dispatch,
-        [jax.ShapeDtypeStruct((rows, width), BF)] + [piece] * len(order),
-        [tokens, norm_gain.reshape(1, width), routing],
-        loads=3,
+        [jax.ShapeDtypeStruct((rows, width), BF), jax.ShapeDtypeStruct((hid, half), BF)] + [piece] * len(order),
+        [tokens, norm_gain.reshape(1, width), routing, w_down],
+        loads=4,
         scratch_shapes=[
             pltpu.VMEM((rows, width), BF),
             pltpu.VMEM((1, width), F32),
             pltpu.VMEM((top, rows), jnp.int32),
-            pltpu.SemaphoreType.DMA((blocks + 2,)),
+            pltpu.SemaphoreType.DMA((blocks + 3,)),
         ],
     )
+    far_down = over_tp(far_half, CORES)
+    last_down = over_tp(far_down, 1)
     arrived = [over_ep(x, s) for x, s in zip(sends, order)]
 
     stored = [routing, gate_weights, w_gate, w_up, shared_gate, shared_up, w_down, shared_down]
@@ -203,25 +210,24 @@
     sums = call(add, [out_piece] * len(keep), [partials[m] for m in keep] + came)
     kept = [sums[0], over_tp(sums[1], CORES)]
 
-    def expert(*refs):
-        mine_ref, came_ref, ws, outs = refs[0], refs[1], refs[2:8], refs[8:]
-        total = [None, None]
-        for wg, wu, wd in (ws[0:3], ws[3:6]):
+    def first(mine_ref, came_ref, *refs):
+        ws, out_ref = refs[:4], refs[4]
+        for i, (wg, wu) in enumerate((ws[:2], ws[2:])):
             gate = dot(mine_ref[...], wg[at_half(False), :]) + dot(came_ref[...], wg[at_half(True), :])
             up = dot(mine_ref[...], wu[at_half(False), :]) + dot(came_ref[...], wu[at_half(True), :])
-            hidden = swiglu(gate, up)
-            for i in range(2):
-                term = dot(hidden, wd[:, at_half(i == 1)])
-                total[i] = term if total[i] is None else total[i] + term
-        for i in range(2):
-            outs[i][...] = total[i].astype(BF)
+            out_ref[:, i * hid : (i + 1) * hid] = swiglu(gate, up)
+
+    def second(mine_ref, came_ref, own_ref, near_ref, far_ref, last_ref, out_ref):
+        total = dot(mine_ref[:, :hid], own_ref[:, at_half(False)]) + dot(mine_ref[:, hid:], near_ref[:, at_half(False)])
+        total = total + dot(came_ref[:, :hid], far_ref[...]) + dot(came_ref[:, hid:], last_ref[...])
+        out_ref[...] = total.astype(BF)
 
     returned = []
     for x, s in zip(arrived, order):
         came = over_tp(x, CORES)
-        mine, other = call(expert, [piece] * 2, [x, came, w_gate, w_up, w_down, near_gate, near_up, near_down])
-        more = over_tp(other, CORES)
-        (out,) = call(add, [piece], [mine, more])
+        hidden = call(first, jax.ShapeDtypeStruct((part, CORES * hid), BF), [x, came, w_gate, w_up, near_gate, near_up])
+        more = over_tp(hidden, CORES)
+        out = call(second, piece, [hidden, more, w_down, near_down, far_down, last_down])
         returned.append(over_ep(out, ep_count - s))
 
     def combine(info_ref, *refs):

time: 69.2 us -> 79.3 us (1.15)
  waiting for transfers between devices: 32.5 us -> 47.8 us
  local copies, waits for them, and re-layouts: 5.09 us -> 0.01 us
  Pallas kernels: 11.1 us -> 12.8 us
  starting transfers between devices: 20 us -> 18.4 us
    ppermute x13 -> x15, waiting for transfers between devices: 5.45 us -> 13.3 us  [over_tp(): return lax.ppermute(x, 'tp', [(i, i ^ m) for i in range(tp_count)])]
    ppermute x6, waiting for transfers between devices: 27 us -> 34.5 us  [over_ep(): lax.ppermute(x, 'ep', [(i, (i + s) % ep_count) for i in range(ep_count)])]
    unnamed x26 -> x6, local copies, waits for them, and re-layouts: 5.09 us -> 0.01 us
    pallas_call x13, Pallas kernels: 11.1 us -> 12.8 us  [call(): pl.pallas_call(kernel, out_shape=outs, in_specs=[pl.BlockSpec(memory_spac...]
    ppermute x13 -> x15, starting transfers between devices: 11.4 us -> 10.1 us  [over_tp(): return lax.ppermute(x, 'tp', [(i, i ^ m) for i in range(tp_count)])]
  transfers between devices with their start and end apart: 19 -> 21, of which waited for: 9 -> 9; matrix products, arithmetic and copies ran while one was open for 0% -> 0% of each run, Pallas kernels for 15% -> 15%
where the time goes in v3:
time: 79.3 us; the launch traced here: 79.1 us
  waiting for transfers between devices  47.8 us (60%)
  starting transfers between devices  18.4 us (23%)
  Pallas kernels  12.8 us (16%)
    ppermute x6, waiting for transfers between devices, over_ep(): lax.ppermute(x, 'ep', [(i, (i + s) % ep_count) for i in range(ep_count)])  34.5 us
    ppermute x15, waiting for transfers between devices, over_tp(): return lax.ppermute(x, 'tp', [(i, i ^ m) for i in range(tp_count)])  13.3 us
    pallas_call x13, Pallas kernels, call(): pl.pallas_call(kernel, out_shape=outs, in_specs=[pl.BlockSpec(memory_spac...  12.8 us
    ppermute x15, starting transfers between devices, over_tp(): return lax.ppermute(x, 'tp', [(i, i ^ m) for i in range(tp_count)])  10.1 us
    ppermute x6, starting transfers between devices, over_ep(): lax.ppermute(x, 'ep', [(i, (i + s) % ep_count) for i in range(ep_count)])  8.24 us
  transfers between devices with their start and end apart: 21, of which 9 were waited for; matrix products, arithmetic and copies ran while one was open for 0% of the time, Pallas kernels for 15%

profile of v3, /device:TPU:0, one launch (start us, length us, event | category | flops | bytes accessed | tf_op | source)
XLA Modules:
  0.0 79.1 jit_solution(12788040616976754628)
XLA Ops:
  0.0 0.5 collective-permute-start.2
  0.5 0.0 collective-permute-start.3
  0.5 0.5 collective-permute-start.5
  1.0 2.2 %shard_map.100 = (bf16[256,2048]{1,0:T(8,128)(2,1)S(1)}, bf16[256,1024]{1,0:T(8,128)(2,1)S(1)}, bf16[96,1024]{1,0:T(8,128)(2,1)S(1)}, bf16[96,1024]{1,0:T(8,128)(2,1)S(1)}, bf16[96,1024]{1,0:T(8,128)(2,1)S(1)}) custom-call(bf16[256,2048]{1,0:T(8,128)(2,1)} %tokens_hbm.1, f32[1,2048]{1,0:T(1,128)} %bitcast.24, s32[2,256]{1,0:T(2,128)} %bitcast.22, ...), custom_call_target="tpu_custom_call" | custom-call | tf_op jit(solution)/shard_map/pallas_call | solution.py:30
  3.3 2.5 %collective-permute-start.6 = (bf16[256,1024]{1,0:T(8,128)(2,1)S(1)}, bf16[256,1024]{1,0:T(8,128)(2,1)S(1)}, u32[]{:S(2)}, u32[]{:S(2)}) collective-permute-start(bf16[256,1024]{1,0:T(8,128)(2,1)S(1)} %get-tuple-element.34), channel_id=1, source_target_pairs={{0,2},{1,3},{2,0},{3,1},{4,6},{5,7},{6,4},{7,5},{8,10},{9,11},{10,... | collective-permute-start | bytes 1572872 | tf_op jit(solution)/shard_map/ppermute | solution.py:75
  5.8 3.6 %collective-permute-start = (bf16[96,1024]{1,0:T(8,128)(2,1)S(1)}, bf16[96,1024]{1,0:T(8,128)(2,1)S(1)}, u32[]{:S(2)}, u32[]{:S(2)}) collective-permute-start(bf16[96,1024]{1,0:T(8,128)(2,1)S(1)} %get-tuple-element.33), channel_id=1, source_target_pairs={{0,12},{4,0},{8,4},{12,8},{1,13},{5,1},{9,5},{13,9},{2,14},{6,2},{... | collective-permute-start | bytes 589832 | tf_op jit(solution)/shard_map/ppermute | solution.py:78
  9.4 4.5 %collective-permute-done.mine_ref = bf16[96,1024]{1,0:T(8,128)(2,1)S(1)} collective-permute-done((bf16[96,1024]{1,0:T(8,128)(2,1)S(1)}, bf16[96,1024]{1,0:T(8,128)(2,1)S(1)}, u32[]{:S(2)}, u32[]{:S(2)}) %collective-permute-start) | collective-permute-done | bytes 196640 | tf_op jit(solution)/shard_map/ppermute | solution.py:78
  14.0 1.5 %collective-permute-start.9 = (bf16[96,1024]{1,0:T(8,128)(2,1)S(1)}, bf16[96,1024]{1,0:T(8,128)(2,1)S(1)}, u32[]{:S(2)}, u32[]{:S(2)}) collective-permute-start(bf16[96,1024]{1,0:T(8,128)(2,1)S(1)} %get-tuple-element.37), channel_id=1, source_target_pairs={{0,8},{4,12},{8,0},{12,4},{1,9},{5,13},{9,1},{13,5},{2,10},{6,14},... | collective-permute-start | bytes 589832 | tf_op jit(solution)/shard_map/ppermute | solution.py:78
  15.4 9.8 %collective-permute-done.9.mine_ref = bf16[96,1024]{1,0:T(8,128)(2,1)S(1)} collective-permute-done((bf16[96,1024]{1,0:T(8,128)(2,1)S(1)}, bf16[96,1024]{1,0:T(8,128)(2,1)S(1)}, u32[]{:S(2)}, u32[]{:S(2)}) %collective-permute-start.9) | collective-permute-done | bytes 196640 | tf_op jit(solution)/shard_map/ppermute | solution.py:78
  25.2 0.0 collective-permute-start.13
  25.2 0.0 collective-permute-done.6.far_ref
  25.3 0.0 collective-permute-start.7
  25.3 7.5 %collective-permute-done.13.mine_ref = bf16[96,1024]{1,0:T(8,128)(2,1)S(1)} collective-permute-done((bf16[96,1024]{1,0:T(8,128)(2,1)S(1)}, bf16[96,1024]{1,0:T(8,128)(2,1)S(1)}, u32[]{:S(2)}, u32[]{:S(2)}) %collective-permute-start.13) | collective-permute-done | bytes 196640 | tf_op jit(solution)/shard_map/ppermute | solution.py:78
  32.7 0.5 collective-permute-start.14
  33.3 6.0 %collective-permute-done.14.came_ref = bf16[96,1024]{1,0:T(8,128)(2,1)S(1)} collective-permute-done((bf16[96,1024]{1,0:T(8,128)(2,1)S(1)}, bf16[96,1024]{1,0:T(8,128)(2,1)S(1)}, u32[]{:S(2)}, u32[]{:S(2)}) %collective-permute-start.14) | collective-permute-done | bytes 196640 | tf_op jit(solution)/shard_map/ppermute | solution.py:75
  39.2 0.5 collective-permute-start.10
  39.8 1.5 %collective-permute-start.1 = (bf16[96,1024]{1,0:T(8,128)(2,1)S(1)}, bf16[96,1024]{1,0:T(8,128)(2,1)S(1)}, u32[]{:S(2)}, u32[]{:S(2)}) collective-permute-start(bf16[96,1024]{1,0:T(8,128)(2,1)S(1)} %collective-permute-done.mine_ref), channel_id=1, source_target_pairs={{0,2},{1,3},{2,0},{3,1},{4,6},{5,7},{6,4},{7,5},{8,10},{9,11},{10,... | collective-permute-start | bytes 589832 | tf_op jit(solution)/shard_map/ppermute | solution.py:75
  41.3 0.0 collective-permute-done.3.refs_3_
  41.3 0.8 %shard_map.106.mine_ref = bf16[96,512]{1,0:T(8,128)(2,1)S(1)} custom-call(bf16[96,1024]{1,0:T(8,128)(2,1)S(1)} %collective-permute-done.13.mine_ref, bf16[96,1024]{1,0:T(8,128)(2,1)S(1)} %collective-permute-done.14.came_ref, bf16[2048,256]{1,0:T(8,128)(2,1)S(1)} %bitcast.14, bf16[2048,256]{1,0:T(8,128)(2,1)S(1)} %bitcast.19, ...), custom_call_target="tpu_custom_call" | custom-call | tf_op jit(solution)/shard_map/pallas_call | solution.py:30
  42.1 0.6 collective-permute-start.15
  42.7 4.3 %collective-permute-done.10.came_ref = bf16[96,1024]{1,0:T(8,128)(2,1)S(1)} collective-permute-done((bf16[96,1024]{1,0:T(8,128)(2,1)S(1)}, bf16[96,1024]{1,0:T(8,128)(2,1)S(1)}, u32[]{:S(2)}, u32[]{:S(2)}) %collective-permute-start.10) | collective-permute-done | bytes 196640 | tf_op jit(solution)/shard_map/ppermute | solution.py:75
  47.0 0.8 %shard_map.104.mine_ref = bf16[96,512]{1,0:T(8,128)(2,1)S(1)} custom-call(bf16[96,1024]{1,0:T(8,128)(2,1)S(1)} %collective-permute-done.9.mine_ref, bf16[96,1024]{1,0:T(8,128)(2,1)S(1)} %collective-permute-done.10.came_ref, bf16[2048,256]{1,0:T(8,128)(2,1)S(1)} %bitcast.15, bf16[2048,256]{1,0:T(8,128)(2,1)S(1)} %bitcast.20, ...), custom_call_target="tpu_custom_call" | custom-call | tf_op jit(solution)/shard_map/pallas_call | solution.py:30
  47.8 0.6 collective-permute-start.11
  48.4 1.5 %collective-permute-done.1.came_ref = bf16[96,1024]{1,0:T(8,128)(2,1)S(1)} collective-permute-done((bf16[96,1024]{1,0:T(8,128)(2,1)S(1)}, bf16[96,1024]{1,0:T(8,128)(2,1)S(1)}, u32[]{:S(2)}, u32[]{:S(2)}) %collective-permute-start.1) | collective-permute-done | bytes 196640 | tf_op jit(solution)/shard_map/ppermute | solution.py:75
  50.0 0.8 %shard_map.102.mine_ref = bf16[96,512]{1,0:T(8,128)(2,1)S(1)} custom-call(bf16[96,1024]{1,0:T(8,128)(2,1)S(1)} %collective-permute-done.mine_ref, bf16[96,1024]{1,0:T(8,128)(2,1)S(1)} %collective-permute-done.1.came_ref, bf16[2048,256]{1,0:T(8,128)(2,1)S(1)} %bitcast.16, bf16[2048,256]{1,0:T(8,128)(2,1)S(1)} %bitcast.21, ...), custom_call_target="tpu_custom_call" | custom-call | tf_op jit(solution)/shard_map/pallas_call | solution.py:30
  50.8 0.6 collective-permute-start.4
  51.4 4.4 %shard_map.101 = (bf16[256,512]{1,0:T(8,128)(2,1)S(1)}, bf16[256,512]{1,0:T(8,128)(2,1)S(1)}, bf16[256,512]{1,0:T(8,128)(2,1)S(1)}, bf16[256,512]{1,0:T(8,128)(2...) custom-call(bf16[256,2048]{1,0:T(8,128)(2,1)S(1)} %get-tuple-element, ...), custom_call_target="tpu_custom_call" | custom-call | tf_op jit(solution)/shard_map/pallas_call | solution.py:30
  55.8 0.0 collective-permute-done.5.near_ref
  55.8 0.1 collective-permute-start.18
  55.9 0.0 collective-permute-done.7.last_ref
  55.9 0.5 collective-permute-start.19
  56.4 0.5 shard_map.107
  56.9 2.5 %collective-permute-start.16 = (bf16[96,1024]{1,0:T(8,128)(2,1)S(1)}, bf16[96,1024]{1,0:T(8,128)(2,1)S(1)}, u32[]{:S(2)}, u32[]{:S(2)}) collective-permute-start(bf16[96,1024]{1,0:T(8,128)(2,1)S(1)} %shard_map.107), channel_id=1, source_target_pairs={{0,12},{4,0},{8,4},{12,8},{1,13},{5,1},{9,5},{13,9},{2,14},{6,2},{... | collective-permute-start | bytes 589832 | tf_op jit(solution)/shard_map/ppermute | solution.py:78
  59.3 0.5 shard_map.105
  59.8 0.1 collective-permute-start.12
  59.9 0.5 shard_map.103
  60.4 0.6 collective-permute-start.8
  61.0 0.0 collective-permute-done.18.refs_2_
  61.0 0.1 shard_map.111
  61.1 1.6 %collective-permute-start.20 = (bf16[256,512]{1,0:T(8,128)(2,1)S(1)}, bf16[256,512]{1,0:T(8,128)(2,1)S(1)}, u32[]{:S(2)}, u32[]{:S(2)}) collective-permute-start(bf16[256,512]{1,0:T(8,128)(2,1)S(1)} %get-tuple-element.52), channel_id=1, source_target_pairs={{0,2},{1,3},{2,0},{3,1},{4,6},{5,7},{6,4},{7,5},{8,10},{9,11},{10,... | collective-permute-start | bytes 786440 | tf_op jit(solution)/shard_map/ppermute | solution.py:75
  62.7 2.5 %collective-permute-done.16.refs_2_ = bf16[96,1024]{1,0:T(8,128)(2,1)S(1)} collective-permute-done((bf16[96,1024]{1,0:T(8,128)(2,1)S(1)}, bf16[96,1024]{1,0:T(8,128)(2,1)S(1)}, u32[]{:S(2)}, u32[]{:S(2)}) %collective-permute-start.16) | collective-permute-done | bytes 196640 | tf_op jit(solution)/shard_map/ppermute | solution.py:78
  65.2 0.4 shard_map.108
  65.7 10.1 %collective-permute-done.12.refs_2_ = bf16[96,1024]{1,0:T(8,128)(2,1)S(1)} collective-permute-done((bf16[96,1024]{1,0:T(8,128)(2,1)S(1)}, bf16[96,1024]{1,0:T(8,128)(2,1)S(1)}, u32[]{:S(2)}, u32[]{:S(2)}) %collective-permute-start.12) | collective-permute-done | bytes 196640 | tf_op jit(solution)/shard_map/ppermute | solution.py:78
  75.8 0.4 shard_map.109
  76.3 0.4 shard_map.110
  76.7 0.1 collective-permute-start.17
  76.8 1.5 %collective-permute-done.17.more_ref = bf16[256,512]{1,0:T(8,128)(2,1)S(1)} collective-permute-done((bf16[256,512]{1,0:T(8,128)(2,1)S(1)}, bf16[256,512]{1,0:T(8,128)(2,1)S(1)}, u32[]{:S(2)}, u32[]{:S(2)}) %collective-permute-start.17) | collective-permute-done | bytes 262176 | tf_op jit(solution)/shard_map/ppermute | solution.py:75
  78.3 0.8 %shard_map.112 = bf16[256,512]{1,0:T(8,128)(2,1)} custom-call(f32[256,512]{1,0:T(8,128)S(1)} %get-tuple-element.45.mine_ref, bf16[256,512]{1,0:T(8,128)(2,1)S(1)} %collective-permute-done.17.more_ref, bf16[256,512]{1,0:T(8,128)(2,1)S(1)} %get-tuple-element.51.near_ref, bf16[256,512]{1,0:T(8,128)(2,1)S(1)} %collective-permute-done.20.far_ref), custom_call_target="tpu_custom_call" | custom-call | tf_op jit(solution)/shard_map/pallas_call | solution.py:30
  (13 shorter events, 0.0 us)
Async XLA Ops:
  0.0 39.8 %collective-permute-start.2 = (bf16[2048,256]{1,0:T(8,128)(2,1)}, bf16[2048,256]{1,0:T(8,128)(2,1)S(1)}, u32[]{:S(2)}, u32[]{:S(2)}) collective-permute-start(bf16[2048,256]{1,0:T(8,128)(2,1)} %bitcast.12), channel_id=1, source_target_pairs={{0,1},{1,0},{2,3},{3,2},{4,5},{5,4},{6,7},{7,6},{8,9},{9,8},{10,11... | collective-permute-start | bytes 3145736 | tf_op jit(solution)/shard_map/ppermute | solution.py:75
  0.5 40.8 %collective-permute-start.3 = (bf16[2048,256]{1,0:T(8,128)(2,1)}, bf16[2048,256]{1,0:T(8,128)(2,1)S(1)}, u32[]{:S(2)}, u32[]{:S(2)}) collective-permute-start(bf16[2048,256]{1,0:T(8,128)(2,1)} %bitcast.17), channel_id=1, source_target_pairs={{0,1},{1,0},{2,3},{3,2},{4,5},{5,4},{6,7},{7,6},{8,9},{9,8},{10,11... | collective-permute-start | bytes 3145736 | tf_op jit(solution)/shard_map/ppermute | solution.py:75
  0.5 55.3 %collective-permute-start.5 = (bf16[256,2048]{1,0:T(8,128)(2,1)}, bf16[256,2048]{1,0:T(8,128)(2,1)S(1)}, u32[]{:S(2)}, u32[]{:S(2)}) collective-permute-start(bf16[256,2048]{1,0:T(8,128)(2,1)} %bitcast.6), channel_id=1, source_target_pairs={{0,1},{1,0},{2,3},{3,2},{4,5},{5,4},{6,7},{7,6},{8,9},{9,8},{10,11... | collective-permute-start | bytes 3145736 | tf_op jit(solution)/shard_map/ppermute | solution.py:75
  1.0 40.3 %copy-start.1 = (bf16[1,2048,256]{2,1,0:T(8,128)(2,1)S(1)}, bf16[1,2048,256]{2,1,0:T(8,128)(2,1)}, u32[]{:S(2)}) copy-start(bf16[1,2048,256]{2,1,0:T(8,128)(2,1)} %param.14) | copy-start | bytes 3145732
  1.0 40.3 %copy-start.2 = (bf16[1,2048,256]{2,1,0:T(8,128)(2,1)S(1)}, bf16[1,2048,256]{2,1,0:T(8,128)(2,1)}, u32[]{:S(2)}) copy-start(bf16[1,2048,256]{2,1,0:T(8,128)(2,1)} %param.15) | copy-start | bytes 3145732
  3.3 22.0 %collective-permute-start.6 = (bf16[256,1024]{1,0:T(8,128)(2,1)S(1)}, bf16[256,1024]{1,0:T(8,128)(2,1)S(1)}, u32[]{:S(2)}, u32[]{:S(2)}) collective-permute-start(bf16[256,1024]{1,0:T(8,128)(2,1)S(1)} %get-tuple-element.34), channel_id=1, source_target_pairs={{0,2},{1,3},{2,0},{3,1},{4,6},{5,7},{6,4},{7,5},{8,10},{9,11},{10,... | collective-permute-start | bytes 1572872 | tf_op jit(solution)/shard_map/ppermute | solution.py:75
  5.8 8.2 %collective-permute-start = (bf16[96,1024]{1,0:T(8,128)(2,1)S(1)}, bf16[96,1024]{1,0:T(8,128)(2,1)S(1)}, u32[]{:S(2)}, u32[]{:S(2)}) collective-permute-start(bf16[96,1024]{1,0:T(8,128)(2,1)S(1)} %get-tuple-element.33), channel_id=1, source_target_pairs={{0,12},{4,0},{8,4},{12,8},{1,13},{5,1},{9,5},{13,9},{2,14},{6,2},{... | collective-permute-start | bytes 589832 | tf_op jit(solution)/shard_map/ppermute | solution.py:78
  14.0 11.3 %collective-permute-start.9 = (bf16[96,1024]{1,0:T(8,128)(2,1)S(1)}, bf16[96,1024]{1,0:T(8,128)(2,1)S(1)}, u32[]{:S(2)}, u32[]{:S(2)}) collective-permute-start(bf16[96,1024]{1,0:T(8,128)(2,1)S(1)} %get-tuple-element.37), channel_id=1, source_target_pairs={{0,8},{4,12},{8,0},{12,4},{1,9},{5,13},{9,1},{13,5},{2,10},{6,14},... | collective-permute-start | bytes 589832 | tf_op jit(solution)/shard_map/ppermute | solution.py:78
  25.2 7.5 %collective-permute-start.13 = (bf16[96,1024]{1,0:T(8,128)(2,1)S(1)}, bf16[96,1024]{1,0:T(8,128)(2,1)S(1)}, u32[]{:S(2)}, u32[]{:S(2)}) collective-permute-start(bf16[96,1024]{1,0:T(8,128)(2,1)S(1)} %get-tuple-element.40), channel_id=1, source_target_pairs={{0,4},{4,8},{8,12},{12,0},{1,5},{5,9},{9,13},{13,1},{2,6},{6,10},{... | collective-permute-start | bytes 589832 | tf_op jit(solution)/shard_map/ppermute | solution.py:78
  25.3 30.6 %collective-permute-start.7 = (bf16[256,1024]{1,0:T(8,128)(2,1)S(1)}, bf16[256,1024]{1,0:T(8,128)(2,1)S(1)}, u32[]{:S(2)}, u32[]{:S(2)}) collective-permute-start(bf16[256,1024]{1,0:T(8,128)(2,1)S(1)} %collective-permute-done.6.far_ref), channel_id=1, source_target_pairs={{0,1},{1,0},{2,3},{3,2},{4,5},{5,4},{6,7},{7,6},{8,9},{9,8},{10,11... | collective-permute-start | bytes 1572872 | tf_op jit(solution)/shard_map/ppermute | solution.py:75
  32.7 6.5 %collective-permute-start.14 = (bf16[96,1024]{1,0:T(8,128)(2,1)S(1)}, bf16[96,1024]{1,0:T(8,128)(2,1)S(1)}, u32[]{:S(2)}, u32[]{:S(2)}) collective-permute-start(bf16[96,1024]{1,0:T(8,128)(2,1)S(1)} %collective-permute-done.13.mine_ref), channel_id=1, source_target_pairs={{0,2},{1,3},{2,0},{3,1},{4,6},{5,7},{6,4},{7,5},{8,10},{9,11},{10,... | collective-permute-start | bytes 589832 | tf_op jit(solution)/shard_map/ppermute | solution.py:75
  39.2 7.8 %collective-permute-start.10 = (bf16[96,1024]{1,0:T(8,128)(2,1)S(1)}, bf16[96,1024]{1,0:T(8,128)(2,1)S(1)}, u32[]{:S(2)}, u32[]{:S(2)}) collective-permute-start(bf16[96,1024]{1,0:T(8,128)(2,1)S(1)} %collective-permute-done.9.mine_ref), channel_id=1, source_target_pairs={{0,2},{1,3},{2,0},{3,1},{4,6},{5,7},{6,4},{7,5},{8,10},{9,11},{10,... | collective-permute-start | bytes 589832 | tf_op jit(solution)/shard_map/ppermute | solution.py:75
  39.8 10.2 %collective-permute-start.1 = (bf16[96,1024]{1,0:T(8,128)(2,1)S(1)}, bf16[96,1024]{1,0:T(8,128)(2,1)S(1)}, u32[]{:S(2)}, u32[]{:S(2)}) collective-permute-start(bf16[96,1024]{1,0:T(8,128)(2,1)S(1)} %collective-permute-done.mine_ref), channel_id=1, source_target_pairs={{0,2},{1,3},{2,0},{3,1},{4,6},{5,7},{6,4},{7,5},{8,10},{9,11},{10,... | collective-permute-start | bytes 589832 | tf_op jit(solution)/shard_map/ppermute | solution.py:75
  42.1 14.3 %collective-permute-start.15 = (bf16[96,512]{1,0:T(8,128)(2,1)S(1)}, bf16[96,512]{1,0:T(8,128)(2,1)S(1)}, u32[]{:S(2)}, u32[]{:S(2)}) collective-permute-start(bf16[96,512]{1,0:T(8,128)(2,1)S(1)} %shard_map.106.mine_ref), channel_id=1, source_target_pairs={{0,2},{1,3},{2,0},{3,1},{4,6},{5,7},{6,4},{7,5},{8,10},{9,11},{10,... | collective-permute-start | bytes 294920 | tf_op jit(solution)/shard_map/ppermute | solution.py:75
  47.8 11.5 %collective-permute-start.11 = (bf16[96,512]{1,0:T(8,128)(2,1)S(1)}, bf16[96,512]{1,0:T(8,128)(2,1)S(1)}, u32[]{:S(2)}, u32[]{:S(2)}) collective-permute-start(bf16[96,512]{1,0:T(8,128)(2,1)S(1)} %shard_map.104.mine_ref), channel_id=1, source_target_pairs={{0,2},{1,3},{2,0},{3,1},{4,6},{5,7},{6,4},{7,5},{8,10},{9,11},{10,... | collective-permute-start | bytes 294920 | tf_op jit(solution)/shard_map/ppermute | solution.py:75
  50.8 9.1 %collective-permute-start.4 = (bf16[96,512]{1,0:T(8,128)(2,1)S(1)}, bf16[96,512]{1,0:T(8,128)(2,1)S(1)}, u32[]{:S(2)}, u32[]{:S(2)}) collective-permute-start(bf16[96,512]{1,0:T(8,128)(2,1)S(1)} %shard_map.102.mine_ref), channel_id=1, source_target_pairs={{0,2},{1,3},{2,0},{3,1},{4,6},{5,7},{6,4},{7,5},{8,10},{9,11},{10,... | collective-permute-start | bytes 294920 | tf_op jit(solution)/shard_map/ppermute | solution.py:75
  51.4 5.0 %copy-start = (bf16[1,256,2048]{2,1,0:T(8,128)(2,1)S(1)}, bf16[1,256,2048]{2,1,0:T(8,128)(2,1)}, u32[]{:S(2)}) copy-start(bf16[1,256,2048]{2,1,0:T(8,128)(2,1)} %param.16) | copy-start | bytes 3145732
  55.8 5.2 %collective-permute-start.18 = (bf16[256,512]{1,0:T(8,128)(2,1)S(1)}, bf16[256,512]{1,0:T(8,128)(2,1)S(1)}, u32[]{:S(2)}, u32[]{:S(2)}) collective-permute-start(bf16[256,512]{1,0:T(8,128)(2,1)S(1)} %get-tuple-element.49), channel_id=1, source_target_pairs={{0,1},{1,0},{2,3},{3,2},{4,5},{5,4},{6,7},{7,6},{8,9},{9,8},{10,11... | collective-permute-start | bytes 786440 | tf_op jit(solution)/shard_map/ppermute | solution.py:75
  55.9 5.1 %collective-permute-start.19 = (bf16[256,512]{1,0:T(8,128)(2,1)S(1)}, bf16[256,512]{1,0:T(8,128)(2,1)S(1)}, u32[]{:S(2)}, u32[]{:S(2)}) collective-permute-start(bf16[256,512]{1,0:T(8,128)(2,1)S(1)} %get-tuple-element.50), channel_id=1, source_target_pairs={{0,1},{1,0},{2,3},{3,2},{4,5},{5,4},{6,7},{7,6},{8,9},{9,8},{10,11... | collective-permute-start | bytes 786440 | tf_op jit(solution)/shard_map/ppermute | solution.py:75
  56.9 8.4 %collective-permute-start.16 = (bf16[96,1024]{1,0:T(8,128)(2,1)S(1)}, bf16[96,1024]{1,0:T(8,128)(2,1)S(1)}, u32[]{:S(2)}, u32[]{:S(2)}) collective-permute-start(bf16[96,1024]{1,0:T(8,128)(2,1)S(1)} %shard_map.107), channel_id=1, source_target_pairs={{0,12},{4,0},{8,4},{12,8},{1,13},{5,1},{9,5},{13,9},{2,14},{6,2},{... | collective-permute-start | bytes 589832 | tf_op jit(solution)/shard_map/ppermute | solution.py:78
  59.8 16.0 %collective-permute-start.12 = (bf16[96,1024]{1,0:T(8,128)(2,1)S(1)}, bf16[96,1024]{1,0:T(8,128)(2,1)S(1)}, u32[]{:S(2)}, u32[]{:S(2)}) collective-permute-start(bf16[96,1024]{1,0:T(8,128)(2,1)S(1)} %shard_map.105), channel_id=1, source_target_pairs={{0,8},{4,12},{8,0},{12,4},{1,9},{5,13},{9,1},{13,5},{2,10},{6,14},... | collective-permute-start | bytes 589832 | tf_op jit(solution)/shard_map/ppermute | solution.py:78
  60.4 15.9 %collective-permute-start.8 = (bf16[96,1024]{1,0:T(8,128)(2,1)S(1)}, bf16[96,1024]{1,0:T(8,128)(2,1)S(1)}, u32[]{:S(2)}, u32[]{:S(2)}) collective-permute-start(bf16[96,1024]{1,0:T(8,128)(2,1)S(1)} %shard_map.103), channel_id=1, source_target_pairs={{0,4},{4,8},{8,12},{12,0},{1,5},{5,9},{9,13},{13,1},{2,6},{6,10},{... | collective-permute-start | bytes 589832 | tf_op jit(solution)/shard_map/ppermute | solution.py:78
  61.1 15.7 %collective-permute-start.20 = (bf16[256,512]{1,0:T(8,128)(2,1)S(1)}, bf16[256,512]{1,0:T(8,128)(2,1)S(1)}, u32[]{:S(2)}, u32[]{:S(2)}) collective-permute-start(bf16[256,512]{1,0:T(8,128)(2,1)S(1)} %get-tuple-element.52), channel_id=1, source_target_pairs={{0,2},{1,3},{2,0},{3,1},{4,6},{5,7},{6,4},{7,5},{8,10},{9,11},{10,... | collective-permute-start | bytes 786440 | tf_op jit(solution)/shard_map/ppermute | solution.py:75
  76.7 1.6 %collective-permute-start.17 = (bf16[256,512]{1,0:T(8,128)(2,1)S(1)}, bf16[256,512]{1,0:T(8,128)(2,1)S(1)}, u32[]{:S(2)}, u32[]{:S(2)}) collective-permute-start(bf16[256,512]{1,0:T(8,128)(2,1)S(1)} %get-tuple-element.46), channel_id=1, source_target_pairs={{0,1},{1,0},{2,3},{3,2},{4,5},{5,4},{6,7},{7,6},{8,9},{9,8},{10,11... | collective-permute-start | bytes 786440 | tf_op jit(solution)/shard_map/ppermute | solution.py:75
